TPU v7x, 32 devices: a whole 2x2x4 slice. The times are simulated.
32 devices in a mesh: sp: 16 (over z, y, x), tp: 2 (over core).
Axes of the slice: x: 2, y: 2, z: 4, core: 2. Of those that a mesh axis runs over, the one named last changes fastest.
Arguments:
- queries: bfloat16 [4096, 512], P('sp', 'tp'), may hold values from -20 to 20
- key_rows: bfloat16 [4096, 512], P('sp', 'tp'), may hold values from -20 to 20
- value_rows: bfloat16 [4096, 512], P('sp', 'tp'), may hold values from -6 to 6
- residual: bfloat16 [4096, 2048], P(('sp', 'tp')), may hold values from -6 to 6
- out_weight: bfloat16 [512, 2048], replicated, may hold values from -0.75 to 0.75
- norm_gain: float32 [2048], replicated, may hold values from 0.1 to 1.9
- routes: int32 [4096, 8], P(('sp', 'tp')), may hold values from 0 to 15, all different within a row; in each aligned block of 128 rows (0 to 127, 128 to 255, ...) at most 80 rows name the same one
- route_weight: float32 [4096, 8], P(('sp', 'tp')), may hold values from 0.1 to 0.6
- expert_gate: bfloat16 [16, 2048, 512], P('sp', None, 'tp'), may hold values from -0.125 to 0.125
- expert_up: bfloat16 [16, 2048, 512], P('sp', None, 'tp'), may hold values from -0.125 to 0.125
- expert_down: bfloat16 [16, 512, 2048], P('sp', 'tp'), may hold values from -0.25 to 0.25
- shared_gate: bfloat16 [2048, 512], replicated, may hold values from -0.125 to 0.125
- shared_up: bfloat16 [2048, 512], replicated, may hold values from -0.125 to 0.125
- shared_down: bfloat16 [512, 2048], replicated, may hold values from -0.25 to 0.25
Outputs:
- output: bfloat16 [4096, 2048], P(('sp', 'tp'))
Inputs may be any that keep to these rules, and one draw needn't show every extreme that they name: `routes`: each row names 8 different experts. In each aligned block of 128 rows (the rows of one device) no expert is named more than 80 times, a bound that some block reaches.
All inputs are finite; a program needn't handle non-finite values.
Results may differ from a plain program's by a relative error of at most 0.012.
Values may be sent and summed in bfloat16 or wider, within the bound.
A program may use at most 192 MiB of HBM per device.

v0:
```python
import functools

import jax
import jax.numpy as jnp
from jax import lax
from jax.experimental import pallas as pl
from jax.experimental.pallas import tpu as pltpu
from jax.sharding import PartitionSpec as P

HEAD_DIM = 64
TOPK = 8


norm_eps = 1e-06


MESH = pl.DeviceIdType.MESH
LANES = 128


def attention_kernel(query_ref, kv_ref, out_ref, acc_ref, later_ref):
    own = lax.axis_index("sp")
    count, width = query_ref.shape
    lane = lax.broadcasted_iota(jnp.int32, (count, LANES), 1)
    row = lax.broadcasted_iota(jnp.int32, (count, count), 0)
    column = lax.broadcasted_iota(jnp.int32, (count, count), 1)
    after = (row > column).astype(jnp.bfloat16)
    acc_ref[...] = jnp.zeros_like(acc_ref)
    later_ref[...] = jnp.zeros_like(later_ref)

    def tile(block, diagonal):
        rows = pl.ds(pl.multiple_of(block * count, count), count)
        for pair in range(width // LANES):
            columns = slice(pair * LANES, (pair + 1) * LANES)
            keys = kv_ref[rows, columns]
            values = kv_ref[rows, width + pair * LANES : width + (pair + 1) * LANES]
            sides = []
            for side in range(LANES // HEAD_DIM):
                head = pair * (LANES // HEAD_DIM) + side
                mine = (lane >= side * HEAD_DIM) & (lane < (side + 1) * HEAD_DIM)
                query = query_ref[:, columns].astype(jnp.float32) * HEAD_DIM ** (-0.5)
                query = jnp.where(mine, query, 0.0).astype(jnp.bfloat16)
                scores = lax.dot_general(
                    query, keys, (((1,), (1,)), ((), ())), preferred_element_type=jnp.float32
                )
                tail = jnp.log(1.0 + jnp.exp(-jnp.abs(scores)))
                cost = jnp.maximum(scores, 0.0) + tail
                if diagonal:
                    cost = jnp.where(column < row, cost, 0.0)
                high = cost.astype(jnp.bfloat16)
                low = (cost - high.astype(jnp.float32)).astype(jnp.bfloat16)
                inside = jnp.dot(high, after, preferred_element_type=jnp.float32)
                inside = inside + jnp.dot(low, after, preferred_element_type=jnp.float32)
                weight = jnp.exp(jnp.minimum(scores, 0.0) - tail - inside)
                if diagonal:
                    weight = jnp.where(column < row, weight, 0.0)
                partial = jnp.dot(
                    weight.astype(jnp.bfloat16), values, preferred_element_type=jnp.float32
                )
                later = later_ref[head]
                sides.append(jnp.exp(-later) * partial)
                total = inside[:, 0:1] + cost[:, 0:1]
                later_ref[head] = later + jnp.broadcast_to(total, later.shape)
            acc_ref[:, columns] += jnp.where(lane < HEAD_DIM, sides[0], sides[1])

    tile(own, True)

    def step(index, carry):
        tile(own - 1 - index, False)
        return carry

    lax.fori_loop(0, own, step, 0)
    out_ref[...] = acc_ref[...].astype(out_ref.dtype)


def attention(queries, kv):
    count, width = queries.shape
    return pl.pallas_call(
        attention_kernel,
        out_shape=jax.ShapeDtypeStruct((count, width), jnp.bfloat16),
        in_specs=[pl.BlockSpec(memory_space=pltpu.VMEM)] * 2,
        out_specs=pl.BlockSpec(memory_space=pltpu.VMEM),
        scratch_shapes=[
            pltpu.VMEM((count, width), jnp.float32),
            pltpu.VMEM((width // HEAD_DIM, count, LANES), jnp.float32),
        ],
        compiler_params=pltpu.CompilerParams(vmem_limit_bytes=56 * 1024 * 1024),
    )(queries, kv)


def gather_kernel(n, depth, in_ref, out_ref, stage, send_sem, recv_sem, local_sem):
    me = lax.axis_index("sp")
    plane = n // depth
    level, place = me // plane, lax.rem(me, plane)

    def above(k):
        return lax.rem(level + k, depth) * plane + place

    def beside(j):
        return level * plane + lax.rem(place + j, plane)

    peers = [above(k) for k in range(1, depth)] + [beside(j) for j in range(1, plane)]
    barrier = pltpu.get_barrier_semaphore()
    for peer in peers:
        pl.semaphore_signal(barrier, inc=1, device_id={"sp": peer}, device_id_type=MESH)
    pl.semaphore_wait(barrier, len(peers))

    def send(source, block, peer, k, j):
        copy = pltpu.make_async_remote_copy(
            src_ref=source,
            dst_ref=out_ref.at[block],
            send_sem=send_sem.at[k, j],
            recv_sem=recv_sem.at[k, j],
            device_id={"sp": peer},
            device_id_type=MESH,
        )
        copy.start()
        return copy

    rising = [send(in_ref, me, above(k), k, 0) for k in range(1, depth)]
    level_copies = [send(in_ref, me, beside(j), 0, j) for j in range(1, plane)]
    inward = pltpu.make_async_copy(in_ref, stage, local_sem)
    inward.start()
    inward.wait()
    outward = pltpu.make_async_copy(stage, out_ref.at[me], local_sem)
    outward.start()
    outward.wait()
    for k in range(1, depth):
        rising[k - 1].wait_recv()
        block = lax.rem(level + depth - k, depth) * plane + place
        for j in range(1, plane):
            level_copies.append(send(out_ref.at[block], block, beside(j), k, j))
    for copy in rising:
        copy.wait_send()
    for copy in level_copies:
        copy.wait()


def gather(array, n, number):
    depth = 4 if n % 4 == 0 else 1
    return pl.pallas_call(
        functools.partial(gather_kernel, n, depth),
        out_shape=jax.ShapeDtypeStruct((n,) + array.shape, array.dtype),
        in_specs=[pl.BlockSpec(memory_space=pltpu.HBM)],
        out_specs=pl.BlockSpec(memory_space=pltpu.HBM),
        scratch_shapes=[
            pltpu.VMEM(array.shape, array.dtype),
            pltpu.SemaphoreType.DMA((depth, n // depth)),
            pltpu.SemaphoreType.DMA((depth, n // depth)),
            pltpu.SemaphoreType.DMA,
        ],
        compiler_params=pltpu.CompilerParams(collective_id=number, has_side_effects=True),
    )(array)


def exchange_kernel(n, in_ref, out_ref, stage, send_sem, recv_sem, local_sem):
    me = lax.axis_index("sp")
    barrier = pltpu.get_barrier_semaphore()
    for k in range(1, n):
        pl.semaphore_signal(
            barrier, inc=1, device_id={"sp": lax.rem(me + k, n)}, device_id_type=MESH
        )
    pl.semaphore_wait(barrier, n - 1)

    def part(peer):
        return in_ref.at[peer]

    copies = []
    for k in range(1, n):
        peer = lax.rem(me + k, n)
        copy = pltpu.make_async_remote_copy(
            src_ref=part(peer),
            dst_ref=out_ref.at[me],
            send_sem=send_sem.at[k],
            recv_sem=recv_sem.at[k],
            device_id={"sp": peer},
            device_id_type=MESH,
        )
        copy.start()
        copies.append(copy)
    inward = pltpu.make_async_copy(part(me), stage, local_sem)
    inward.start()
    inward.wait()
    outward = pltpu.make_async_copy(stage, out_ref.at[me], local_sem)
    outward.start()
    outward.wait()
    for copy in copies:
        copy.wait()


def exchange(array, n, number):
    shape = array.shape[1:]
    return pl.pallas_call(
        functools.partial(exchange_kernel, n),
        out_shape=jax.ShapeDtypeStruct((n,) + shape, array.dtype),
        in_specs=[pl.BlockSpec(memory_space=pltpu.HBM)],
        out_specs=pl.BlockSpec(memory_space=pltpu.HBM),
        scratch_shapes=[
            pltpu.VMEM(shape, array.dtype),
            pltpu.SemaphoreType.DMA((n,)),
            pltpu.SemaphoreType.DMA((n,)),
            pltpu.SemaphoreType.DMA,
        ],
        compiler_params=pltpu.CompilerParams(collective_id=number, has_side_effects=True),
    )(array)


def expert_product(rows, gate_half, up_half, down_half):
    gate = jnp.einsum("seid,edf->seif", rows, gate_half, preferred_element_type=jnp.float32)
    upward = jnp.einsum("seid,edf->seif", rows, up_half, preferred_element_type=jnp.float32)
    hidden = (jax.nn.silu(gate) * upward).astype(jnp.bfloat16)
    return jnp.einsum("seif,efd->seid", hidden, down_half, preferred_element_type=jnp.float32)


def local(
    queries,
    key_rows,
    value_rows,
    residual,
    out_weight,
    norm_gain,
    routes,
    route_weight,
    expert_gate,
    expert_up,
    expert_down,
    shared_gate,
    shared_up,
    shared_down,
):
    query_count = queries.shape[0]
    local_width = queries.shape[1]
    blocks = lax.axis_size("sp")
    kv = jnp.concatenate([key_rows, value_rows], axis=1)
    kv = gather(kv, blocks, 0).reshape(-1, kv.shape[1])
    attended = attention(queries, kv)
    token_rows = residual.shape[0]
    weight_rows = lax.dynamic_slice_in_dim(
        out_weight, lax.axis_index("tp") * local_width, local_width, 0
    )
    projected = lax.psum_scatter(
        jnp.dot(attended, weight_rows, preferred_element_type=jnp.float32),
        "tp",
        scatter_dimension=0,
        tiled=True,
    )
    mixed_wide = (residual.astype(jnp.float32) + projected).astype(jnp.bfloat16).astype(jnp.float32)
    inverse = lax.rsqrt(jnp.mean(mixed_wide * mixed_wide, axis=1, keepdims=True) + norm_eps)
    normed = (mixed_wide * inverse * norm_gain).astype(jnp.bfloat16)
    width = normed.shape[1]
    local_experts = expert_gate.shape[0]
    experts_all = blocks * local_experts
    capacity = max(2, token_rows * TOPK * 5 // (4 * experts_all))
    flat_routes = routes.reshape(-1)
    picks = (flat_routes[:, None] == jnp.arange(experts_all, dtype=jnp.int32)[None, :]).astype(
        jnp.int32
    )
    earlier = jnp.cumsum(picks, axis=0) - picks
    position = flat_routes * capacity + jnp.sum(earlier * picks, axis=1)
    filler = (
        jnp.zeros((experts_all * capacity,), jnp.int32)
        .at[position]
        .set(jnp.arange(flat_routes.shape[0], dtype=jnp.int32) + 1)
    )
    occupied = filler > 0
    source_token = jnp.maximum(filler - 1, 0) // TOPK
    outgoing = jnp.where(
        occupied[:, None], normed[source_token], jnp.zeros((), jnp.bfloat16)
    ).reshape(experts_all, capacity, width)
    both = lax.all_gather(
        exchange(
            outgoing.reshape(blocks, local_experts * capacity, width), blocks, 1
        ).reshape(outgoing.shape),
        "tp",
        axis=0,
        tiled=True,
    )
    shaped = both.reshape(-1, local_experts, both.shape[1], both.shape[2])
    pieces = expert_product(shaped, expert_gate, expert_up, expert_down).reshape(both.shape)
    summed = lax.psum_scatter(pieces.astype(jnp.bfloat16), "tp", scatter_dimension=0, tiled=True)
    results = exchange(
        summed.reshape(blocks, local_experts * capacity, width), blocks, 2
    ).reshape(
        experts_all * capacity, width
    )
    picked = results[position].reshape(token_rows, TOPK, width)
    routed = jnp.sum(picked.astype(jnp.float32) * route_weight[:, :, None], axis=1)
    shared_gate_out = jnp.dot(normed, shared_gate, preferred_element_type=jnp.float32)
    shared_up_out = jnp.dot(normed, shared_up, preferred_element_type=jnp.float32)
    shared_act = (jax.nn.silu(shared_gate_out) * shared_up_out).astype(jnp.bfloat16)
    shared_out = jnp.dot(shared_act, shared_down, preferred_element_type=jnp.float32)
    return (mixed_wide + routed + shared_out).astype(jnp.bfloat16)


def solution(mesh):
    return jax.shard_map(
        local,
        mesh=mesh,
        in_specs=(
            P("sp", "tp"),
            P("sp", "tp"),
            P("sp", "tp"),
            P(("sp", "tp"), None),
            P(),
            P(),
            P(("sp", "tp"), None),
            P(("sp", "tp"), None),
            P("sp", None, "tp"),
            P("sp", None, "tp"),
            P("sp", "tp", None),
            P(),
            P(),
            P(),
        ),
        out_specs=P(("sp", "tp"), None),
        check_vma=False,
    )
```

profile of v0, /device:TPU:15, one launch (start us, length us, event | category | flops | bytes accessed | tf_op | source)
XLA Modules:
  0.0 495.3 jit_solution(1531325682605833697)
XLA Ops:
  6.5 0.0 copy-start
  6.5 0.0 reduce-scatter.3.cloned.1.call-start
  6.5 1.8 pad_maximum_fusion.in_ref
  8.4 48.4 %shard_map.136 = bf16[16,256,512]{2,1,0:T(8,128)(2,1)} custom-call(bf16[256,512]{1,0:T(8,128)(2,1)} %pad_maximum_fusion.in_ref), custom_call_target="tpu_custom_call" | custom-call | tf_op jit(solution)/shard_map/pallas_call | solution.py:141
  56.8 18.1 %shard_map.137 = bf16[256,256]{1,0:T(8,128)(2,1)} custom-call(bf16[256,256]{1,0:T(8,128)(2,1)} %query_ref.1, bf16[4096,512]{1,0:T(8,128)(2,1)} %bitcast.84), custom_call_target="tpu_custom_call" | custom-call | tf_op jit(solution)/shard_map/pallas_call | solution.py:78
  74.9 0.0 copy-done
  74.9 0.0 copy-start.5
  74.9 0.0 copy-start.3
  74.9 2.8 fusion.17
  77.7 0.0 copy-start.4
  77.7 0.0 reduce-scatter.3.cloned.1.call-update
  77.7 0.0 all-gather.2.cloned.1.call-start
  77.8 0.0 copy-done.5
  77.8 0.1 copy.25
  77.9 0.1 eq.29
  78.0 0.1 eq.25
  78.1 4.5 reduce-window.6
  82.6 0.1 slice.12
  82.7 0.1 copy.27
  82.8 0.1 copy.28
  82.9 0.1 copy.24
  83.0 0.1 mul.66
  83.1 0.1 broadcast_add_fusion
  83.3 4.3 scatter_custom_fusion
  87.6 0.1 broadcast_in_dim.24
  87.7 18.1 %reduce-scatter.3.cloned.1.call-done = f32[128,2048]{1,0:T(8,128)} async-done(((f32[256,2048]{1,0:T(8,128)}), f32[128,2048]{1,0:T(8,128)}) %reduce-scatter.3.cloned.1.call-update) | async-done | bytes 1048592 | tf_op jit(solution)/shard_map/reduce_scatter | solution.py:241
  105.8 0.0 copy-done.3
  105.8 1.5 fusion.9
  107.3 0.0 copy-done.4
  107.3 0.2 fusion.11
  107.5 6.1 %gather_fusion = bf16[1280,2048]{1,0:T(8,128)(2,1)} fusion(bf16[128,2048]{1,0:T(8,128)(2,1)S(1)} %fusion.11, s32[2048]{0:T(1024)S(1)} %pad_clamp_fusion), kind=kCustom, calls=%fused_computation | custom fusion | bytes 10490880 | tf_op jit(solution)/shard_map/gather | solution.py:268
  113.6 5.2 %broadcast_select_fusion.in_ref = bf16[16,80,2048]{2,1,0:T(8,128)(2,1)} fusion(bf16[16,80,2048]{2,1,0:T(8,128)(2,1)} %bitcast.83, pred[16,80]{1,0:T(8,128)(4,1)S(1)} %broadcast_in_dim.24), kind=kLoop, calls=%fused_computation.6 | loop fusion | flops 2621440 | bytes 10487040 | tf_op jit(solution)/shard_map/jit(_where)/select_n | solution.py:267
  118.9 139.8 %shard_map.138 = bf16[16,80,2048]{2,1,0:T(8,128)(2,1)} custom-call(bf16[16,80,2048]{2,1,0:T(8,128)(2,1)} %broadcast_select_fusion.in_ref), custom_call_target="tpu_custom_call" | custom-call | tf_op jit(solution)/shard_map/pallas_call | solution.py:193
  258.6 0.0 copy-start.7
  258.6 0.0 all-gather.2.cloned.1.call-update
  258.7 0.0 copy-start.8
  258.7 0.0 reduce-scatter.5.cloned.1.call-start
  258.7 22.4 %all-gather.2.cloned.1.call-done = bf16[32,80,2048]{2,1,0:T(8,128)(2,1)} async-done(((bf16[16,80,2048]{2,1,0:T(8,128)(2,1)}), bf16[32,80,2048]{2,1,0:T(8,128)(2,1)}) %all-gather.2.cloned.1.call-update) | async-done | bytes 10485776 | tf_op jit(solution)/shard_map/all_gather | solution.py:270
  281.1 0.0 copy-done.7
  281.1 8.4 %fusion.13 = f32[32,80,256]{2,1,0:T(8,128)} fusion(bf16[32,80,2048]{2,1,0:T(8,128)(2,1)} %all-gather.2.cloned.1.call-done, bf16[1,2048,256]{2,1,0:T(8,128)(2,1)S(1)} %copy-done.7), kind=kOutput, calls=%fused_computation.27 | convolution fusion | flops 2684354560 | bytes 14155776 | tf_op jit(solution)/shard_map/seid,edf->seif/dot_general | solution.py:210
  289.5 0.0 copy-done.8
  289.5 16.2 %convolution_convert_fusion = bf16[32,80,2048]{2,1,0:T(8,128)(2,1)} fusion(f32[32,80,256]{2,1,0:T(8,128)} %fusion.13, bf16[32,80,2048]{2,1,0:T(8,128)(2,1)} %all-gather.2.cloned.1.call-done, bf16[1,256,2048]{2,1,0:T(8,128)(2,1)S(1)} %copy-done.8, bf16[1,2048,256]{2,1,0:T(8,128)(2,1)} %param.22), kind=kOutput, calls=%fused_computation.5 | convolution fusion | flops 5377884160 | bytes 25690112 | tf_op jit(solution)/shard_map/seif,efd->seid/dot_general | solution.py:212
  305.7 0.0 copy-start.6
  305.7 0.0 copy-start.2
  305.7 0.0 reduce-scatter.5.cloned.1.call-update
  305.8 0.7 copy-done.6
  306.4 0.1 copy.29
  306.5 0.8 copy-done.2
  307.3 0.5 fusion.37
  307.8 17.2 %reduce-scatter.5.cloned.1.call-done.in_ref = bf16[16,80,2048]{2,1,0:T(8,128)(2,1)} async-done(((bf16[32,80,2048]{2,1,0:T(8,128)(2,1)}), bf16[16,80,2048]{2,1,0:T(8,128)(2,1)}) %reduce-scatter.5.cloned.1.call-update) | async-done | bytes 5242896 | tf_op jit(solution)/shard_map/reduce_scatter | solution.py:280
  325.1 139.9 %shard_map.139 = bf16[16,80,2048]{2,1,0:T(8,128)(2,1)} custom-call(bf16[16,80,2048]{2,1,0:T(8,128)(2,1)} %reduce-scatter.5.cloned.1.call-done.in_ref), custom_call_target="tpu_custom_call" | custom-call | tf_op jit(solution)/shard_map/pallas_call | solution.py:193
  465.0 12.0 %gather_fusion.1 = bf16[1024,2048]{1,0:T(8,128)(2,1)} fusion(bf16[1280,2048]{1,0:T(8,128)(2,1)} %bitcast.82, s32[1024]{0:T(1024)S(1)} %broadcast_clamp_fusion), kind=kCustom, calls=%fused_computation.1 | custom fusion | bytes 8392704 | tf_op jit(solution)/shard_map/gather | solution.py:286
  477.0 0.0 copy-start.1
  477.0 7.6 %fusion = f32[128,2048]{1,0:T(8,128)} fusion(bf16[1024,2048]{1,0:T(8,128)(2,1)} %gather_fusion.1, f32[128,8]{1,0:T(8,128)S(1)} %copy.29), kind=kLoop, calls=%fused_computation.4 | loop fusion | flops 6029312 | bytes 5246976 | tf_op jit(solution)/shard_map/reduce_sum | solution.py:287
  484.6 4.2 fusion.5
  488.8 0.0 copy-done.1
  (12 shorter events, 0.1 us)
Async XLA Ops:
  6.5 68.4 %copy-start = (bf16[512,2048]{1,0:T(8,128)(2,1)S(1)}, bf16[512,2048]{1,0:T(8,128)(2,1)}, u32[]{:S(2)}) copy-start(bf16[512,2048]{1,0:T(8,128)(2,1)} %param.18) | copy-start | bytes 6291460
  6.5 99.3 %reduce-scatter.3.cloned.1.call-start = ((), (), s32[]{:S(2)}) async-start(), calls=%async_computation.2 | async-start | bytes 3145728 | tf_op jit(solution)/shard_map/reduce_scatter | solution.py:241
  74.9 2.8 copy-start.5
  74.9 30.9 %copy-start.3 = (bf16[128,2048]{1,0:T(8,128)(2,1)S(1)}, bf16[128,2048]{1,0:T(8,128)(2,1)}, u32[]{:S(2)}) copy-start(bf16[128,2048]{1,0:T(8,128)(2,1)} %param.17) | copy-start | bytes 1572868
  77.7 29.6 %copy-start.4 = (f32[2048]{0:T(1024)S(1)}, f32[2048]{0:T(1024)}, u32[]{:S(2)}) copy-start(f32[2048]{0:T(1024)} %param.19) | copy-start | bytes 24580
  77.7 203.4 %all-gather.2.cloned.1.call-start = ((), (), s32[]{:S(2)}) async-start(), calls=%async_computation.3 | async-start | bytes 15728640 | tf_op jit(solution)/shard_map/all_gather | solution.py:270
  258.6 22.5 %copy-start.7 = (bf16[1,2048,256]{2,1,0:T(8,128)(2,1)S(1)}, bf16[1,2048,256]{2,1,0:T(8,128)(2,1)}, u32[]{:S(2)}) copy-start(bf16[1,2048,256]{2,1,0:T(8,128)(2,1)} %param.23) | copy-start | bytes 3145732
  258.7 30.8 %copy-start.8 = (bf16[1,256,2048]{2,1,0:T(8,128)(2,1)S(1)}, bf16[1,256,2048]{2,1,0:T(8,128)(2,1)}, u32[]{:S(2)}) copy-start(bf16[1,256,2048]{2,1,0:T(8,128)(2,1)} %param.24) | copy-start | bytes 3145732
  258.7 66.4 %reduce-scatter.5.cloned.1.call-start = ((), (), s32[]{:S(2)}) async-start(), calls=%async_computation.4 | async-start | bytes 15728640 | tf_op jit(solution)/shard_map/reduce_scatter | solution.py:280
  305.7 0.7 copy-start.6
  305.7 1.6 copy-start.2
  477.0 11.8 %copy-start.1 = (bf16[512,2048]{1,0:T(8,128)(2,1)S(1)}, bf16[512,2048]{1,0:T(8,128)(2,1)}, u32[]{:S(2)}) copy-start(bf16[512,2048]{1,0:T(8,128)(2,1)} %param.18) | copy-start | bytes 6291460
Sparse Core Ops, SparseCore 0:
  77.8 27.9 reduce-scatter.2
  258.8 22.2 all-gather.1
  305.9 19.1 reduce-scatter.4
where the time goes:
time: 496 us; the launch traced here: 495 us
  Pallas kernels  346 us (70%)
  waiting for transfers between devices  57.7 us (12%)
  matrix products  32.1 us (6%)
  local copies, waits for them, and re-layouts  24.9 us (5%)
  other arithmetic  21 us (4%)
  between operations  13.3 us (3%)
    pallas_call x2, Pallas kernels, exchange(): pl.pallas_call(functools.partial(exchange_kernel, n), out_shape=jax.Shape...  280 us
    pallas_call x1, Pallas kernels, gather(): pl.pallas_call(functools.partial(gather_kernel, n, depth), out_shape=jax....  48.4 us
    all_gather x1, waiting for transfers between devices, local(): lax.all_gather(exchange(outgoing.reshape(blocks, local_experts * capacity...  22.4 us
    pallas_call x1, Pallas kernels, attention(): pl.pallas_call(attention_kernel, out_shape=jax.ShapeDtypeStruct((count, w...  18.1 us
    reduce_scatter x1, waiting for transfers between devices, local(): lax.psum_scatter(jnp.dot(attended, weight_rows, preferred_element_type=jn...  18.1 us
    reduce_scatter x1, waiting for transfers between devices, local(): lax.psum_scatter(pieces.astype(jnp.bfloat16), 'tp', scatter_dimension=0,...  17.2 us
    dot_general x1, matrix products, expert_product(): jnp.einsum('seif,efd->seid', hidden, down_half, preferred_element_type=jn...  16.2 us
    gather x1, local copies, waits for them, and re-layouts, local(): picked = results[position].reshape(token_rows, TOPK, width)  12 us
  transfers between devices with their start and end apart: 3, of which 3 were waited for; matrix products, arithmetic and copies ran while one was open for 2% of the time, Pallas kernels for 0%

commit v1 on v0

--- a/solution.py
+++ b/solution.py
@@ -203,6 +203,364 @@
         ],
         compiler_params=pltpu.CompilerParams(collective_id=number, has_side_effects=True),
     )(array)
+
+
+LEVELS = 4
+
+
+def level_at(z, p):
+    low = z * 2 < LEVELS
+    place = jnp.where(low, z, LEVELS - 1 - z)
+    step = jnp.where(p == 0, place, jnp.where(p - 1 < place, p - 1, p))
+    return jnp.where(low, step, LEVELS - 1 - step)
+
+
+def expert_kernel(
+    pieces,
+    normed_ref,
+    mixed_ref,
+    weight_ref,
+    *refs,
+):
+    halves = [refs[3 * j : 3 * j + 3] for j in range(4)]
+    shared = refs[12:15]
+    out_ref = refs[15]
+    (tok, acc, wg, wu, wd, sg, su, sd, shared_out, hidden, shared_hidden) = refs[16:27]
+    (y_out, y_in, z_out, z_in, route) = refs[27:32]
+    (load_sem, w_send, w_recv, zs_sem, zr_sem, ys_sem, yr_sem) = refs[32:39]
+    (rys_sem, ryr_sem, rzs_sem, rzr_sem) = refs[39:43]
+    me = lax.axis_index("sp")
+    x, y, z = lax.rem(me, 2), lax.rem(me // 2, 2), me // 4
+    count, width = normed_ref.shape
+    experts = weight_ref.shape[0]
+    half = wg.shape[2]
+    rows = count // pieces
+
+    def chip(level, side):
+        return level * 4 + side * 2 + x
+
+    loads = []
+    for j in range(4):
+        loads.append((halves[j][0], wg.at[j]))
+        loads.append((halves[j][1], wu.at[j]))
+        loads.append((halves[j][2], wd.at[pl.ds(j * half, half)]))
+    loads = list(zip(shared, (sg, su, sd))) + loads
+    loads = [
+        pltpu.make_async_copy(source, target, load_sem.at[k])
+        for k, (source, target) in enumerate(loads)
+    ]
+    for load in loads:
+        load.start()
+
+    barrier = pltpu.get_barrier_semaphore()
+    peers = [(dz, r) for dz in range(LEVELS) for r in range(2) if (dz, r) != (0, 0)]
+    for dz, r in peers:
+        peer = chip(lax.rem(z + dz, LEVELS), lax.rem(y + r, 2))
+        pl.semaphore_signal(barrier, inc=1, device_id={"sp": peer}, device_id_type=MESH)
+    pl.semaphore_wait(barrier, len(peers))
+
+    def remote(source, target, send, recv, peer):
+        return pltpu.make_async_remote_copy(
+            src_ref=source,
+            dst_ref=target,
+            send_sem=send,
+            recv_sem=recv,
+            device_id={"sp": peer},
+            device_id_type=MESH,
+        )
+
+    def part(c):
+        return pl.ds(c * rows, rows)
+
+    beside = chip(z, 1 - y)
+    above, below = me + 4, me - 4
+
+    def along(source, t, c, up):
+        return remote(
+            source,
+            tok.at[t, 0, part(c)],
+            zs_sem.at[0 if up else 1, t, c],
+            zr_sem.at[t, c],
+            above if up else below,
+        )
+
+    def across(source, t, c):
+        return remote(
+            source, tok.at[t, 1, part(c)], ys_sem.at[t, c], yr_sem.at[t, c], beside
+        )
+
+    def spread(source, t, c):
+        @pl.when((t <= z) & (z < LEVELS - 1))
+        def _():
+            along(source, t, c, True).start()
+
+        @pl.when((t >= z) & (z > 0))
+        def _():
+            along(source, t, c, False).start()
+
+        across(source, t, c).start()
+
+    for c in range(pieces):
+        spread(normed_ref.at[part(c)], z, c)
+
+    def route_copy(dz, r, incoming):
+        origin = lax.rem(z + LEVELS - dz, LEVELS) if incoming else z
+        peer = chip(lax.rem(z + dz, LEVELS), lax.rem(y + r, 2))
+        return remote(
+            weight_ref, route.at[origin * 2 + r], w_send.at[dz, r], w_recv.at[dz, r], peer
+        )
+
+    for dz, r in peers:
+        route_copy(dz, r, False).start()
+    route[z * 2] = weight_ref[...]
+    tok[z, 0] = normed_ref[...]
+
+    for load in loads[:3]:
+        load.wait()
+    span = min(width, 512)
+    shared_half = sg.shape[1] // 2
+    for j in range(2):
+        columns = slice(j * shared_half, (j + 1) * shared_half)
+        gate = jnp.dot(normed_ref[...], sg[:, columns], preferred_element_type=jnp.float32)
+        upward = jnp.dot(normed_ref[...], su[:, columns], preferred_element_type=jnp.float32)
+        shared_hidden[:, columns] = (jax.nn.silu(gate) * upward).astype(jnp.bfloat16)
+
+    def shared_step(k, carry):
+        columns = pl.ds(pl.multiple_of(k * span, span), span)
+        shared_out[:, columns] = mixed_ref[:, columns].astype(jnp.float32) + jnp.dot(
+            shared_hidden[...], sd[:, columns], preferred_element_type=jnp.float32
+        )
+        return carry
+
+    lax.fori_loop(0, width // span, shared_step, 0)
+
+    for dz, r in peers:
+        route_copy(dz, r, True).wait_recv()
+    for load in loads[3:]:
+        load.wait()
+
+    def forward(p):
+        t = level_at(z, p)
+        for c in range(pieces):
+            remote(
+                normed_ref.at[part(c)], tok.at[t, 0, part(c)], zs_sem.at[0, t, c],
+                zr_sem.at[t, c], beside,
+            ).wait_recv()
+            spread(tok.at[t, 0, part(c)], t, c)
+
+    lane = lax.broadcasted_iota(jnp.int32, (count, LANES), 1)
+
+    def column(slot, expert):
+        table = jnp.concatenate(
+            [route[slot], jnp.zeros((LANES - experts, count), jnp.float32)], axis=0
+        )
+        picked = jnp.where(lane == expert, jnp.transpose(table), 0.0)
+        return jnp.sum(picked, axis=1, keepdims=True)
+
+    def give(t):
+        for c in range(pieces):
+            remote(
+                y_out.at[t, part(c)], y_in.at[t, part(c)], rys_sem.at[t, c],
+                ryr_sem.at[t, c], beside,
+            ).start()
+
+    def step(i, carry):
+        @pl.when(i == 0)
+        def _():
+            forward(1)
+            forward(2)
+
+        @pl.when(i == 1)
+        def _():
+            forward(3)
+
+        t = level_at(z, i)
+        for c in range(pieces):
+            across(normed_ref.at[part(c)], t, c).wait_recv()
+        sides = [
+            jnp.concatenate([column(t * 2, e), column(t * 2 + 1, e)], axis=0)
+            for e in (me, me + 1 - 2 * x)
+        ]
+
+        def inner(j, carry):
+            block = tok[t].reshape(2 * count, width)
+            gate = jnp.dot(block, wg[j], preferred_element_type=jnp.float32)
+            upward = jnp.dot(block, wu[j], preferred_element_type=jnp.float32)
+            scale = jnp.where(j < 2, sides[0], sides[1])
+            columns = pl.ds(pl.multiple_of(j * half, half), half)
+            hidden[:, columns] = (jax.nn.silu(gate) * upward * scale).astype(jnp.bfloat16)
+            return carry
+
+        lax.fori_loop(0, 4, inner, 0)
+
+        def outer(k, carry):
+            columns = pl.ds(pl.multiple_of(k * span, span), span)
+            result = jnp.dot(hidden[...], wd[:, columns], preferred_element_type=jnp.float32)
+            acc[t, :, columns] = result[:count]
+            y_out[t, :, columns] = result[count:].astype(jnp.bfloat16)
+            return carry
+
+        lax.fori_loop(0, width // span, outer, 0)
+
+        @pl.when(i == 2)
+        def _():
+            give(level_at(z, 2))
+
+        @pl.when(i == 3)
+        def _():
+            give(level_at(z, 3))
+            give(level_at(z, 1))
+            give(level_at(z, 0))
+
+        return carry
+
+    lax.fori_loop(0, LEVELS, step, 0)
+
+    def take(t, c):
+        remote(
+            y_out.at[t, part(c)], y_in.at[t, part(c)], rys_sem.at[t, c],
+            ryr_sem.at[t, c], beside,
+        ).wait_recv()
+
+    def arrive(slot, c):
+        remote(
+            z_out.at[0, part(c)], z_in.at[slot, part(c)], rzs_sem.at[0, c],
+            rzr_sem.at[slot, c], beside,
+        ).wait_recv()
+
+    def hop(p, c):
+        t = level_at(z, p)
+        up = t > z
+        slot = jnp.where(up | (t < z - 1), t, LEVELS)
+        return remote(
+            z_out.at[t, part(c)],
+            z_in.at[slot, part(c)],
+            rzs_sem.at[t, c],
+            rzr_sem.at[slot, c],
+            jnp.where(up, above, below),
+        )
+
+    for p in (2, 3, 1):
+        t = level_at(z, p)
+        up = t > z
+        fed = (up & (z > 0)) | (jnp.logical_not(up) & (z < LEVELS - 1))
+        for c in range(pieces):
+            take(t, c)
+
+            @pl.when(fed)
+            def _():
+                arrive(t, c)
+                z_out[t, part(c)] = (
+                    acc[t, part(c)]
+                    + y_in[t, part(c)].astype(jnp.float32)
+                    + z_in[t, part(c)].astype(jnp.float32)
+                ).astype(jnp.bfloat16)
+
+            @pl.when(jnp.logical_not(fed))
+            def _():
+                z_out[t, part(c)] = (
+                    acc[t, part(c)] + y_in[t, part(c)].astype(jnp.float32)
+                ).astype(jnp.bfloat16)
+
+            hop(p, c).start()
+
+    for c in range(pieces):
+        shared_out[part(c)] += acc[z, part(c)]
+
+        @pl.when(z > 0)
+        def _():
+            arrive(z, c)
+            shared_out[part(c)] += z_in[z, part(c)].astype(jnp.float32)
+
+        @pl.when(z < LEVELS - 1)
+        def _():
+            arrive(LEVELS, c)
+            shared_out[part(c)] += z_in[LEVELS, part(c)].astype(jnp.float32)
+
+        take(z, c)
+        out_ref[part(c)] = (
+            shared_out[part(c)] + y_in[z, part(c)].astype(jnp.float32)
+        ).astype(out_ref.dtype)
+
+    for dz, r in peers:
+        route_copy(dz, r, False).wait_send()
+
+    def drain(t, carry):
+        for c in range(pieces):
+            @pl.when((t <= z) & (z < LEVELS - 1))
+            def _():
+                along(tok.at[t, 0, part(c)], t, c, True).wait_send()
+
+            @pl.when((t >= z) & (z > 0))
+            def _():
+                along(tok.at[t, 0, part(c)], t, c, False).wait_send()
+
+            across(tok.at[t, 0, part(c)], t, c).wait_send()
+            remote(
+                y_out.at[t, part(c)], y_in.at[t, part(c)], rys_sem.at[t, c],
+                ryr_sem.at[t, c], beside,
+            ).wait_send()
+        return carry
+
+    lax.fori_loop(0, LEVELS, drain, 0)
+    for p in (1, 2, 3):
+        for c in range(pieces):
+            hop(p, c).wait_send()
+
+
+def expert_layer(normed, mixed, weights, halves, shared, number):
+    count, width = normed.shape
+    half = halves[0][0].shape[1]
+    middle = shared[0].shape[1]
+    pieces = 4
+    flat = [array for trio in halves for array in trio] + list(shared)
+    vmem, hbm = pl.BlockSpec(memory_space=pltpu.VMEM), pl.BlockSpec(memory_space=pl.ANY)
+    bf16, f32 = jnp.bfloat16, jnp.float32
+    dma = pltpu.SemaphoreType.DMA
+    return pl.pallas_call(
+        functools.partial(expert_kernel, pieces),
+        out_shape=jax.ShapeDtypeStruct((count, width), bf16),
+        in_specs=[vmem] * 3 + [hbm] * len(flat),
+        out_specs=vmem,
+        scratch_shapes=[
+            pltpu.VMEM((LEVELS, 2, count, width), bf16),
+            pltpu.VMEM((LEVELS, count, width), f32),
+            pltpu.VMEM((4, width, half), bf16),
+            pltpu.VMEM((4, width, half), bf16),
+            pltpu.VMEM((4 * half, width), bf16),
+            pltpu.VMEM((width, middle), bf16),
+            pltpu.VMEM((width, middle), bf16),
+            pltpu.VMEM((middle, width), bf16),
+            pltpu.VMEM((count, width), f32),
+            pltpu.VMEM((2 * count, 4 * half), bf16),
+            pltpu.VMEM((count, middle), bf16),
+            pltpu.VMEM((LEVELS, count, width), bf16),
+            pltpu.VMEM((LEVELS, count, width), bf16),
+            pltpu.VMEM((LEVELS, count, width), bf16),
+            pltpu.VMEM((LEVELS + 1, count, width), bf16),
+            pltpu.VMEM((2 * LEVELS,) + weights.shape, f32),
+            dma((len(flat),)),
+            dma((LEVELS, 2)),
+            dma((LEVELS, 2)),
+            dma((2, LEVELS, pieces)),
+            dma((LEVELS, pieces)),
+            dma((LEVELS, pieces)),
+            dma((LEVELS, pieces)),
+            dma((LEVELS, pieces)),
+            dma((LEVELS, pieces)),
+            dma((LEVELS, pieces)),
+            dma((LEVELS + 1, pieces)),
+        ],
+        compiler_params=pltpu.CompilerParams(
+            collective_id=number,
+            has_side_effects=True,
+            vmem_limit_bytes=60 * 1024 * 1024,
+        ),
+    )(normed, mixed, weights, *flat)
+
+
+def swapped(array, axis, size):
+    return lax.ppermute(array, axis, [(i, i ^ 1) for i in range(size)])
 
 
 def expert_product(rows, gate_half, up_half, down_half):
@@ -250,6 +608,21 @@
     width = normed.shape[1]
     local_experts = expert_gate.shape[0]
     experts_all = blocks * local_experts
+    if blocks == 4 * LEVELS and local_experts == 1 and lax.axis_size("tp") == 2:
+        own = [expert_gate[0], expert_up[0], expert_down[0]]
+        other = [swapped(array, "tp", 2) for array in own]
+        near = [swapped(array, "sp", blocks) for array in own]
+        far = [swapped(array, "tp", 2) for array in near]
+        picked = routes[:, :, None] == jnp.arange(experts_all, dtype=jnp.int32)
+        table = jnp.sum(jnp.where(picked, route_weight[:, :, None], 0.0), axis=1)
+        return expert_layer(
+            normed,
+            mixed_wide.astype(jnp.bfloat16),
+            table.T,
+            (own, other, near, far),
+            (shared_gate, shared_up, shared_down),
+            1,
+        )
     capacity = max(2, token_rows * TOPK * 5 // (4 * experts_all))
     flat_routes = routes.reshape(-1)
     picks = (flat_routes[:, None] == jnp.arange(experts_all, dtype=jnp.int32)[None, :]).astype(

time: 496 us -> 280 us (0.56)
  Pallas kernels: 346 us -> 180 us
  matrix products: 32.1 us -> 2.77 us
  local copies, waits for them, and re-layouts: 24.9 us -> 3.84 us
  other arithmetic: 21 us -> 5.03 us
  starting transfers between devices: 0.09 us -> 14.8 us
    pallas_call x2 -> x1, Pallas kernels: 280 us -> 113 us  [expert_layer(): pl.pallas_call(functools.partial(expert_kernel, pieces), out_shape=jax.Sh...]
    ppermute x0 -> x9, waiting for transfers between devices: none -> 55.9 us  [swapped(): return lax.ppermute(array, axis, [(i, i ^ 1) for i in range(size)])]
    dot_general x4 -> x0, matrix products: 29.3 us -> none  [the longest x1 16.2 us: expert_product(): jnp.einsum('seif,efd->seid', hidden, down_half, preferred_element_type=jn...]
    all_gather x1 -> x0, waiting for transfers between devices: 22.4 us -> none  [local(): lax.all_gather(exchange(outgoing.reshape(blocks, local_experts * capacity...]
    gather x2 -> x0, local copies, waits for them, and re-layouts: 18.1 us -> none  [the longest x1 12 us: local(): picked = results[position].reshape(token_rows, TOPK, width)]
    reduce_scatter x1, waiting for transfers between devices: 18.1 us -> 0.01 us  [local(): lax.psum_scatter(jnp.dot(attended, weight_rows, preferred_element_type=jn...]
    reduce_scatter x1 -> x0, waiting for transfers between devices: 17.2 us -> none  [local(): lax.psum_scatter(pieces.astype(jnp.bfloat16), 'tp', scatter_dimension=0,...]
    ppermute x0 -> x9, starting transfers between devices: none -> 14.8 us  [swapped(): return lax.ppermute(array, axis, [(i, i ^ 1) for i in range(size)])]
  transfers between devices with their start and end apart: 3 -> 10, of which waited for: 3 -> 3; matrix products, arithmetic and copies ran while one was open for 2% -> 1% of each run, Pallas kernels for 0% -> 0%
where the time goes in v1:
time: 280 us; the launch traced here: 276 us
  Pallas kernels  180 us (64%)
  waiting for transfers between devices  55.9 us (20%)
  starting transfers between devices  14.8 us (5%)
  between operations  13.5 us (5%)
  other arithmetic  5.03 us (2%)
  local copies, waits for them, and re-layouts  3.84 us (1%)
    pallas_call x1, Pallas kernels, expert_layer(): pl.pallas_call(functools.partial(expert_kernel, pieces), out_shape=jax.Sh...  113 us
    ppermute x9, waiting for transfers between devices, swapped(): return lax.ppermute(array, axis, [(i, i ^ 1) for i in range(size)])  55.9 us
    pallas_call x1, Pallas kernels, gather(): pl.pallas_call(functools.partial(gather_kernel, n, depth), out_shape=jax....  48.4 us
    pallas_call x1, Pallas kernels, attention(): pl.pallas_call(attention_kernel, out_shape=jax.ShapeDtypeStruct((count, w...  18.1 us
    ppermute x9, starting transfers between devices, swapped(): return lax.ppermute(array, axis, [(i, i ^ 1) for i in range(size)])  14.8 us
  transfers between devices with their start and end apart: 10, of which 3 were waited for; matrix products, arithmetic and copies ran while one was open for 1% of the time, Pallas kernels for 0%

profile of v1, /device:TPU:15, one launch (start us, length us, event | category | flops | bytes accessed | tf_op | source)
XLA Modules:
  0.0 275.7 jit_solution(15460573333035224219)
XLA Ops:
  6.5 0.0 copy-start
  6.5 0.0 reduce-scatter.2.cloned.1.call-start
  6.5 1.8 pad_maximum_fusion.in_ref
  8.4 48.4 %shard_map.136 = bf16[16,256,512]{2,1,0:T(8,128)(2,1)} custom-call(bf16[256,512]{1,0:T(8,128)(2,1)} %pad_maximum_fusion.in_ref), custom_call_target="tpu_custom_call" | custom-call | tf_op jit(solution)/shard_map/pallas_call | solution.py:141
  56.8 18.1 %shard_map.137 = bf16[256,256]{1,0:T(8,128)(2,1)} custom-call(bf16[256,256]{1,0:T(8,128)(2,1)} %query_ref.1, bf16[4096,512]{1,0:T(8,128)(2,1)} %bitcast.6), custom_call_target="tpu_custom_call" | custom-call | tf_op jit(solution)/shard_map/pallas_call | solution.py:78
  74.9 0.0 copy-done
  74.9 0.0 copy-start.2
  74.9 0.0 copy-start.6
  74.9 0.0 copy-start.7
  74.9 2.8 %fusion.3 = f32[256,2048]{1,0:T(8,128)} fusion(bf16[256,256]{1,0:T(8,128)(2,1)} %shard_map.137, bf16[512,2048]{1,0:T(8,128)(2,1)S(1)} %copy-done, s32[]{:T(128)S(6)} %select_n.7), kind=kOutput, calls=%fused_computation.6 | convolution fusion | flops 268435456 | bytes 3276804 | tf_op jit(solution)/shard_map/dot_general | solution.py:600
  77.7 0.0 copy-start.5
  77.7 0.0 reduce-scatter.2.cloned.1.call-update
  77.7 0.0 copy-done.2
  77.8 0.1 collective-permute-start.3
  77.8 1.5 collective-permute-start.4
  79.3 0.1 collective-permute-start.5
  79.4 2.1 collective-permute-start
  81.5 0.0 collective-permute-start.1
  81.5 19.7 %collective-permute-done.3.refs_6_ = bf16[2048,256]{1,0:T(8,128)(2,1)} collective-permute-done((bf16[2048,256]{1,0:T(8,128)(2,1)S(1)}, bf16[2048,256]{1,0:T(8,128)(2,1)}, u32[]{:S(2)}, u32[]{:S(2)}) %collective-permute-start.3) | collective-permute-done | bytes 1048608 | tf_op jit(solution)/shard_map/ppermute | solution.py:563
  101.1 4.4 %collective-permute-start.2 = (bf16[256,2048]{1,0:T(8,128)(2,1)}, bf16[256,2048]{1,0:T(8,128)(2,1)}, u32[]{:S(2)}, u32[]{:S(2)}) collective-permute-start(bf16[256,2048]{1,0:T(8,128)(2,1)} %bitcast.14), channel_id=1, source_target_pairs={{0,1},{1,0},{2,3},{3,2},{4,5},{5,4},{6,7},{7,6},{8,9},{9,8},{10,11... | collective-permute-start | bytes 3145736 | tf_op jit(solution)/shard_map/ppermute | solution.py:563
  105.5 18.1 %collective-permute-done.4.refs_7_ = bf16[2048,256]{1,0:T(8,128)(2,1)} collective-permute-done((bf16[2048,256]{1,0:T(8,128)(2,1)}, bf16[2048,256]{1,0:T(8,128)(2,1)}, u32[]{:S(2)}, u32[]{:S(2)}) %collective-permute-start.4) | collective-permute-done | bytes 1048608 | tf_op jit(solution)/shard_map/ppermute | solution.py:563
  123.6 4.4 %collective-permute-start.6 = (bf16[2048,256]{1,0:T(8,128)(2,1)}, bf16[2048,256]{1,0:T(8,128)(2,1)}, u32[]{:S(2)}, u32[]{:S(2)}) collective-permute-start(bf16[2048,256]{1,0:T(8,128)(2,1)} %collective-permute-done.3.refs_6_), channel_id=1, source_target_pairs={{0,1},{1,0},{2,3},{3,2},{4,5},{5,4},{6,7},{7,6},{8,9},{9,8},{10,11... | collective-permute-start | bytes 3145736 | tf_op jit(solution)/shard_map/ppermute | solution.py:563
  128.0 18.1 %collective-permute-done.5.refs_8_ = bf16[256,2048]{1,0:T(8,128)(2,1)} collective-permute-done((bf16[256,2048]{1,0:T(8,128)(2,1)}, bf16[256,2048]{1,0:T(8,128)(2,1)}, u32[]{:S(2)}, u32[]{:S(2)}) %collective-permute-start.5) | collective-permute-done | bytes 1048608 | tf_op jit(solution)/shard_map/ppermute | solution.py:563
  146.1 2.4 collective-permute-start.7
  148.4 0.0 collective-permute-done.refs_3_
  148.4 0.0 copy-start.3
  148.4 1.0 copy-done.3
  149.4 0.0 collective-permute-start.8
  149.4 0.0 copy-done.6
  149.4 0.0 copy-done.7
  149.4 0.6 select_reduce_fusion
  150.0 0.0 reduce-scatter.2.cloned.1.call-done
  150.0 1.6 fusion
  151.6 0.0 copy-start.1
  151.6 0.0 copy-done.5
  151.7 1.0 fusion.2.normed_ref
  152.6 0.0 collective-permute-done.1.refs_4_
  152.6 0.0 collective-permute-done.2.refs_5_
  152.7 0.0 collective-permute-done.6.refs_9_
  152.7 0.0 collective-permute-done.7.refs_10_
  152.7 0.0 collective-permute-done.8.refs_11_
  152.7 0.0 copy-start.4
  152.7 0.0 copy-done.1
  152.7 1.0 copy-done.4
  153.7 113.3 %shard_map.138 = bf16[128,2048]{1,0:T(8,128)(2,1)} custom-call(bf16[128,2048]{1,0:T(8,128)(2,1)} %fusion.2.normed_ref, bf16[128,2048]{1,0:T(8,128)(2,1)} %copy-done.1, f32[16,128]{1,0:T(8,128)} %bitcast.16, bf16[2048,256]{1,0:T(8,128)(2,1)} %bitcast.7, bf16[2048,256]{1,0:T(8,128)(2,1)} %bitcast.12, bf16[256,2048]{1,0:T(8,128)(2,1)} %bitcast.15, ...), custom_call_target="tpu_custom_call" | custom-call | tf_op jit(solution)/shard_map/pallas_call | solution.py:520
  266.9 1.9 copy.18
  (1 shorter events, 0.0 us)
Async XLA Ops:
  6.5 68.4 %copy-start = (bf16[512,2048]{1,0:T(8,128)(2,1)S(1)}, bf16[512,2048]{1,0:T(8,128)(2,1)}, u32[]{:S(2)}) copy-start(bf16[512,2048]{1,0:T(8,128)(2,1)} %param.18) | copy-start | bytes 6291460
  6.5 143.5 %reduce-scatter.2.cloned.1.call-start = ((), (), s32[]{:S(2)}) async-start(), calls=%async_computation.1 | async-start | bytes 3145728 | tf_op jit(solution)/shard_map/reduce_scatter | solution.py:599
  74.9 2.8 %copy-start.2 = (bf16[1,2048,256]{2,1,0:T(8,128)(2,1)S(1)}, bf16[1,2048,256]{2,1,0:T(8,128)(2,1)}, u32[]{:S(2)}) copy-start(bf16[1,2048,256]{2,1,0:T(8,128)(2,1)} %param.22) | copy-start | bytes 3145732
  74.9 74.5 %copy-start.6 = (f32[128,8]{0,1:T(8,128)S(1)}, f32[128,8]{0,1:T(8,128)}, u32[]{:S(2)}) copy-start(f32[128,8]{0,1:T(8,128)} %param.21) | copy-start | bytes 12292
  74.9 74.5 %copy-start.7 = (s32[128,8]{0,1:T(8,128)S(1)}, s32[128,8]{0,1:T(8,128)}, u32[]{:S(2)}) copy-start(s32[128,8]{0,1:T(8,128)} %param.20) | copy-start | bytes 12292
  77.7 73.9 %copy-start.5 = (f32[2048]{0:T(1024)S(1)}, f32[2048]{0:T(1024)}, u32[]{:S(2)}) copy-start(f32[2048]{0:T(1024)} %param.19) | copy-start | bytes 24580
  77.8 23.4 %collective-permute-start.3 = (bf16[2048,256]{1,0:T(8,128)(2,1)S(1)}, bf16[2048,256]{1,0:T(8,128)(2,1)}, u32[]{:S(2)}, u32[]{:S(2)}) collective-permute-start(bf16[2048,256]{1,0:T(8,128)(2,1)S(1)} %bitcast.8), channel_id=1, source_target_pairs={{0,2},{2,0},{4,6},{6,4},{8,10},{10,8},{12,14},{14,12},{16,18},{18,... | collective-permute-start | bytes 3145736 | tf_op jit(solution)/shard_map/ppermute | solution.py:563
  77.8 45.7 %collective-permute-start.4 = (bf16[2048,256]{1,0:T(8,128)(2,1)}, bf16[2048,256]{1,0:T(8,128)(2,1)}, u32[]{:S(2)}, u32[]{:S(2)}) collective-permute-start(bf16[2048,256]{1,0:T(8,128)(2,1)} %bitcast.10), channel_id=1, source_target_pairs={{0,2},{2,0},{4,6},{6,4},{8,10},{10,8},{12,14},{14,12},{16,18},{18,... | collective-permute-start | bytes 3145736 | tf_op jit(solution)/shard_map/ppermute | solution.py:563
  79.3 66.8 %collective-permute-start.5 = (bf16[256,2048]{1,0:T(8,128)(2,1)}, bf16[256,2048]{1,0:T(8,128)(2,1)}, u32[]{:S(2)}, u32[]{:S(2)}) collective-permute-start(bf16[256,2048]{1,0:T(8,128)(2,1)} %bitcast.13), channel_id=1, source_target_pairs={{0,2},{2,0},{4,6},{6,4},{8,10},{10,8},{12,14},{14,12},{16,18},{18,... | collective-permute-start | bytes 3145736 | tf_op jit(solution)/shard_map/ppermute | solution.py:563
  79.4 69.1 %collective-permute-start = (bf16[2048,256]{1,0:T(8,128)(2,1)S(1)}, bf16[2048,256]{1,0:T(8,128)(2,1)S(1)}, u32[]{:S(2)}, u32[]{:S(2)}) collective-permute-start(bf16[2048,256]{1,0:T(8,128)(2,1)S(1)} %bitcast.9), channel_id=1, source_target_pairs={{0,1},{1,0},{2,3},{3,2},{4,5},{5,4},{6,7},{7,6},{8,9},{9,8},{10,11... | collective-permute-start | bytes 3145736 | tf_op jit(solution)/shard_map/ppermute | solution.py:563
  81.5 71.2 %collective-permute-start.1 = (bf16[2048,256]{1,0:T(8,128)(2,1)}, bf16[2048,256]{1,0:T(8,128)(2,1)}, u32[]{:S(2)}, u32[]{:S(2)}) collective-permute-start(bf16[2048,256]{1,0:T(8,128)(2,1)} %bitcast.11), channel_id=1, source_target_pairs={{0,1},{1,0},{2,3},{3,2},{4,5},{5,4},{6,7},{7,6},{8,9},{9,8},{10,11... | collective-permute-start | bytes 3145736 | tf_op jit(solution)/shard_map/ppermute | solution.py:563
  101.1 51.5 %collective-permute-start.2 = (bf16[256,2048]{1,0:T(8,128)(2,1)}, bf16[256,2048]{1,0:T(8,128)(2,1)}, u32[]{:S(2)}, u32[]{:S(2)}) collective-permute-start(bf16[256,2048]{1,0:T(8,128)(2,1)} %bitcast.14), channel_id=1, source_target_pairs={{0,1},{1,0},{2,3},{3,2},{4,5},{5,4},{6,7},{7,6},{8,9},{9,8},{10,11... | collective-permute-start | bytes 3145736 | tf_op jit(solution)/shard_map/ppermute | solution.py:563
  123.6 29.1 %collective-permute-start.6 = (bf16[2048,256]{1,0:T(8,128)(2,1)}, bf16[2048,256]{1,0:T(8,128)(2,1)}, u32[]{:S(2)}, u32[]{:S(2)}) collective-permute-start(bf16[2048,256]{1,0:T(8,128)(2,1)} %collective-permute-done.3.refs_6_), channel_id=1, source_target_pairs={{0,1},{1,0},{2,3},{3,2},{4,5},{5,4},{6,7},{7,6},{8,9},{9,8},{10,11... | collective-permute-start | bytes 3145736 | tf_op jit(solution)/shard_map/ppermute | solution.py:563
  146.1 6.6 %collective-permute-start.7 = (bf16[2048,256]{1,0:T(8,128)(2,1)}, bf16[2048,256]{1,0:T(8,128)(2,1)}, u32[]{:S(2)}, u32[]{:S(2)}) collective-permute-start(bf16[2048,256]{1,0:T(8,128)(2,1)} %collective-permute-done.4.refs_7_), channel_id=1, source_target_pairs={{0,1},{1,0},{2,3},{3,2},{4,5},{5,4},{6,7},{7,6},{8,9},{9,8},{10,11... | collective-permute-start | bytes 3145736 | tf_op jit(solution)/shard_map/ppermute | solution.py:563
  148.4 1.0 copy-start.3
  149.4 3.3 %collective-permute-start.8 = (bf16[256,2048]{1,0:T(8,128)(2,1)}, bf16[256,2048]{1,0:T(8,128)(2,1)S(1)}, u32[]{:S(2)}, u32[]{:S(2)}) collective-permute-start(bf16[256,2048]{1,0:T(8,128)(2,1)} %collective-permute-done.5.refs_8_), channel_id=1, source_target_pairs={{0,1},{1,0},{2,3},{3,2},{4,5},{5,4},{6,7},{7,6},{8,9},{9,8},{10,11... | collective-permute-start | bytes 3145736 | tf_op jit(solution)/shard_map/ppermute | solution.py:563
  151.6 1.1 copy-start.1
  152.7 1.0 copy-start.4
Sparse Core Ops, SparseCore 0:
  77.9 27.9 reduce-scatter.1

commit v2 on v0

--- a/solution.py
+++ b/solution.py
@@ -205,6 +205,721 @@
     )(array)
 
 
+LEVELS = 4
+WEIGHT_CUTS = 4
+
+
+def level_at(z, p):
+    low = z * 2 < LEVELS
+    place = jnp.where(low, z, LEVELS - 1 - z)
+    step = jnp.where(p == 0, place, jnp.where(p - 1 < place, p - 1, p))
+    return jnp.where(low, step, LEVELS - 1 - step)
+
+
+def layer_kernel(pieces, names, *refs):
+    s = dict(zip(names, refs))
+    f32, bf16 = jnp.float32, jnp.bfloat16
+    me, core = lax.axis_index("sp"), lax.axis_index("tp")
+    x, y, z = lax.rem(me, 2), lax.rem(me // 2, 2), me // 4
+    out_ref = s["out"]
+    count, width = out_ref.shape
+    tokens = s["query"].shape[0]
+    blocks = s["kv"].shape[0]
+    experts = s["table"].shape[0]
+    half = s["wg"].shape[2]
+    rows = count // pieces
+    span = min(width, 512)
+
+    def chip(level, side, place):
+        return level * 4 + side * 2 + place
+
+    def remote(source, target, send, recv, peer, peer_core=None):
+        return pltpu.make_async_remote_copy(
+            src_ref=source,
+            dst_ref=target,
+            send_sem=send,
+            recv_sem=recv,
+            device_id={"sp": peer, "tp": core if peer_core is None else peer_core},
+            device_id_type=MESH,
+        )
+
+    pair = me + 1 - 2 * x
+    beside = chip(z, 1 - y, x)
+    above, below = me + 4, me - 4
+    mirror = chip(LEVELS - 1 - z, 1 - y, 0)
+
+    def landed(target, recv):
+        remote(target, target, s["idle"].at[0], recv, beside).wait_recv()
+
+    wg, wu, wd = s["wg"], s["wu"], s["wd"]
+
+    def trio(j):
+        return wg.at[j], wu.at[j], wd.at[pl.ds(j * half, half)]
+
+    loads = list(zip((s["gate"], s["up"], s["down"]), trio(0)))
+    loads += [(s["project"], s["wo"])]
+    loads += list(zip((s["shared_gate"], s["shared_up"], s["shared_down"]), (s["sg"], s["su"], s["sd"])))
+    loads = [
+        pltpu.make_async_copy(source, target, s["load_sem"].at[k])
+        for k, (source, target) in enumerate(loads)
+    ]
+    for load in loads:
+        load.start()
+
+    def lanes(place):
+        return pl.ds(pl.multiple_of(place * LANES, LANES), LANES)
+
+    kv = s["kv"]
+    near = [
+        pltpu.make_async_copy(s[name].at[:, lanes(x)], kv.at[me, k], s["near_sem"].at[k])
+        for k, name in enumerate(("key", "value"))
+    ]
+    for copy in near:
+        copy.start()
+
+    barrier = pltpu.get_barrier_semaphore()
+    peers = [(dz, r) for dz in range(LEVELS) for r in range(2) if (dz, r) != (0, 0)]
+    greeted = [
+        (chip(lax.rem(z + dz, LEVELS), lax.rem(y + r, 2), x), core) for dz, r in peers
+    ]
+    greeted += [(me, 1 - core), (pair, core), (pair, 1 - core)]
+    greeted += [(mirror + x, 1 - core), (mirror + 1 - x, core), (mirror + 1 - x, 1 - core)]
+    for peer, peer_core in greeted:
+        pl.semaphore_signal(
+            barrier, inc=1, device_id={"sp": peer, "tp": peer_core}, device_id_type=MESH
+        )
+    pl.semaphore_wait(barrier, len(greeted))
+
+    swaps = [
+        remote(
+            s[name].at[:, lanes(1 - x)], kv.at[me, k], s["kxs"].at[k], s["kxr"].at[k], pair
+        )
+        for k, name in enumerate(("key", "value"))
+    ]
+    for copy in swaps:
+        copy.start()
+
+    query, qs = s["query"], s["qs"]
+    kept = pltpu.make_async_copy(query.at[:, lanes(0)], qs.at[0], s["near_sem"].at[2])
+
+    def query_send(place):
+        keep = remote(
+            query.at[:, lanes(1)], qs.at[0], s["qss"].at[1], s["qsr"].at[0], pair
+        )
+        move = remote(
+            query.at[:, lanes(place)], qs.at[1], s["qss"].at[place], s["qsr"].at[1],
+            mirror + place,
+        )
+        return keep, move
+
+    @pl.when(x == 0)
+    def _():
+        kept.start()
+        query_send(1)[0].start()
+
+    @pl.when(x == 1)
+    def _():
+        query_send(0)[1].start()
+        query_send(1)[1].start()
+
+    def kv_along(b, up):
+        return remote(
+            kv.at[b], kv.at[b], s["kzs"].at[0 if up else 1, b], s["kzr"].at[b],
+            above if up else below,
+        )
+
+    def kv_across(b):
+        return remote(kv.at[b], kv.at[b], s["kys"].at[b], s["kyr"].at[b], beside)
+
+    def kv_spread(b):
+        t = b // 4
+
+        @pl.when((t <= z) & (z < LEVELS - 1))
+        def _():
+            kv_along(b, True).start()
+
+        @pl.when((t >= z) & (z > 0))
+        def _():
+            kv_along(b, False).start()
+
+        kv_across(b).start()
+
+    for copy in near:
+        copy.wait()
+    kv_spread(me)
+
+    def route_copy(dz, r, incoming):
+        origin = lax.rem(z + LEVELS - dz, LEVELS) if incoming else z
+        peer = chip(lax.rem(z + dz, LEVELS), lax.rem(y + r, 2), x)
+        return remote(
+            s["table"], s["route"].at[origin * 2 + r], s["w_send"].at[dz, r],
+            s["w_recv"].at[dz, r], peer,
+        )
+
+    for dz, r in peers:
+        route_copy(dz, r, False).start()
+    s["route"][z * 2] = s["table"][...]
+
+    for load in loads[:3]:
+        load.wait()
+
+    def core_copy(j, a):
+        k = 3 * (j // 2) + a
+        return remote(
+            trio(j)[a], trio(j + 1)[a], s["wts"].at[k], s["wtr"].at[k], me, 1 - core
+        )
+
+    def weight_piece(k):
+        a, r = k // WEIGHT_CUTS, k % WEIGHT_CUTS
+        source, target = trio(0)[a], trio(2)[a]
+        size = source.shape[0] // WEIGHT_CUTS
+        cut = pl.ds(r * size, size)
+        return remote(source.at[cut], target.at[cut], s["wxs"].at[k], s["wxr"].at[k], pair)
+
+    for a in range(3):
+        core_copy(0, a).start()
+    for k in range(2):
+        weight_piece(k).start()
+
+    row = lax.broadcasted_iota(jnp.int32, (tokens, tokens), 0)
+    column = lax.broadcasted_iota(jnp.int32, (tokens, tokens), 1)
+    s["after"][...] = (row > column).astype(bf16)
+    s["seg"][...] = jnp.zeros_like(s["seg"])
+    s["sum"][...] = jnp.zeros_like(s["sum"])
+
+    for k in range(2):
+        landed(kv.at[pair, k], s["kxr"].at[k])
+    kv_spread(pair)
+
+    @pl.when(x == 0)
+    def _():
+        kept.wait()
+
+    @pl.when(x == 1)
+    def _():
+        landed(qs.at[0], s["qsr"].at[0])
+
+    landed(qs.at[1], s["qsr"].at[1])
+    lane = lax.broadcasted_iota(jnp.int32, (tokens, LANES), 1)
+    first = lane < HEAD_DIM
+    for f in range(2):
+        scaled = qs[f].astype(f32) * HEAD_DIM ** (-0.5)
+        s["qm"][f, 0] = jnp.where(first, scaled, 0.0).astype(bf16)
+        s["qm"][f, 1] = jnp.where(first, 0.0, scaled).astype(bf16)
+
+    def kv_forward(p):
+        t = level_at(z, p)
+        for k in range(2):
+            b = chip(t, y, k)
+            landed(kv.at[b], s["kzr"].at[b])
+            kv_spread(b)
+
+    def tile(f, t, b, diagonal):
+        parts, totals = [], []
+        for h in range(2):
+            scores = lax.dot_general(
+                s["qm"][f, h], kv[b, 0], (((1,), (1,)), ((), ())), preferred_element_type=f32
+            )
+            tail = jnp.log(1.0 + jnp.exp(-jnp.abs(scores)))
+            cost = jnp.maximum(scores, 0.0) + tail
+            if diagonal:
+                mask = lax.broadcasted_iota(
+                    jnp.int32, (tokens, tokens), 1
+                ) < lax.broadcasted_iota(jnp.int32, (tokens, tokens), 0)
+                cost = jnp.where(mask, cost, 0.0)
+            high = cost.astype(bf16)
+            low = (cost - high.astype(f32)).astype(bf16)
+            inside = jnp.dot(high, s["after"][...], preferred_element_type=f32)
+            inside = inside + jnp.dot(low, s["after"][...], preferred_element_type=f32)
+            weight = jnp.exp(jnp.minimum(scores, 0.0) - tail - inside)
+            if diagonal:
+                weight = jnp.where(mask, weight, 0.0)
+            parts.append(jnp.dot(weight.astype(bf16), kv[b, 1], preferred_element_type=f32))
+            totals.append(inside[:, 0:1] + cost[:, 0:1])
+        total = jnp.where(first, totals[0], totals[1])
+        s["seg"][f, t] = s["seg"][f, t] * jnp.exp(-total) + jnp.where(first, parts[0], parts[1])
+        s["sum"][f, t] += total
+
+    kept_block = chip(z, y, 0)
+
+    def attend(i, carry):
+        @pl.when(i == 0)
+        def _():
+            kv_forward(1)
+            kv_forward(2)
+
+        @pl.when(i == 1)
+        def _():
+            kv_forward(3)
+
+        t = level_at(z, i)
+        for k in range(2):
+            b = chip(t, 1 - y, k)
+            landed(kv.at[b], s["kyr"].at[b])
+
+        def one_query(f, carry):
+            block = jnp.where(f == 0, kept_block, blocks - 1 - kept_block)
+            full = jnp.clip(block - 4 * t, 0, 4)
+
+            def one_key(b, carry):
+                tile(f, t, 4 * t + b, False)
+                return carry
+
+            lax.fori_loop(0, full, one_key, 0)
+
+            @pl.when((block >= 4 * t) & (block < 4 * t + 4))
+            def _():
+                tile(f, t, block, True)
+
+            return carry
+
+        lax.fori_loop(0, 2, one_query, 0)
+
+        @pl.when(i == 0)
+        def _():
+            weight_piece(2).start()
+            weight_piece(3).start()
+
+        @pl.when(i == 1)
+        def _():
+            weight_piece(4).start()
+
+        @pl.when(i == 2)
+        def _():
+            weight_piece(5).start()
+
+        return carry
+
+    lax.fori_loop(0, LEVELS, attend, 0)
+
+    for f in range(2):
+        later = s["sum"][f, LEVELS - 1]
+        value = s["seg"][f, LEVELS - 1]
+        for t in reversed(range(LEVELS - 1)):
+            value = value + jnp.exp(-later) * s["seg"][f, t]
+            later = later + s["sum"][f, t]
+        s["ob"][f] = value.astype(bf16)
+
+    spot = core * 2 + x
+
+    def attended_copy(f, d):
+        other = lax.rem(core + d, 2)
+        source = s["ob"].at[f, pl.ds(pl.multiple_of(other * count, count), count)]
+        target = kept_block if f == 0 else mirror + 1
+        return remote(
+            source, s["att"].at[spot], s["oss"].at[f, d], s["osr"].at[spot], target, other
+        )
+
+    attended_copy(1, 0).start()
+    attended_copy(1, 1).start()
+    attended_copy(0, 1).start()
+
+    @pl.when(x == 1)
+    def _():
+        attended_copy(0, 0).start()
+
+    @pl.when(x == 0)
+    def _():
+        s["att"][spot] = s["ob"][0, pl.ds(pl.multiple_of(core * count, count), count)]
+
+    loads[3].wait()
+    for k in range(4):
+        @pl.when((x == 1) | (k != spot))
+        def _():
+            landed(s["att"].at[k], s["osr"].at[k])
+
+    for k in range(6, 3 * WEIGHT_CUTS):
+        weight_piece(k).start()
+
+    mixed, normed = s["mixed"], s["normed"]
+    attended = jnp.concatenate([s["att"][k] for k in range(4)], axis=1)
+
+    def project_step(k, carry):
+        columns = pl.ds(pl.multiple_of(k * span, span), span)
+        value = s["residual"][:, columns].astype(f32) + jnp.dot(
+            attended, s["wo"][:, columns], preferred_element_type=f32
+        )
+        value = value.astype(bf16)
+        mixed[:, columns] = value
+        value = value.astype(f32)
+        return carry + jnp.sum(value * value, axis=1, keepdims=True)
+
+    squares = lax.fori_loop(0, width // span, project_step, jnp.zeros((count, 1), f32))
+    inverse = lax.rsqrt(squares / width + norm_eps)
+    for k in range(width // span):
+        columns = slice(k * span, (k + 1) * span)
+        normed[:, columns] = (
+            mixed[:, columns].astype(f32) * inverse * s["gain"][:, columns]
+        ).astype(bf16)
+
+    tok, acc = s["tok"], s["acc"]
+    y_out, y_in, z_out, z_in = s["y_out"], s["y_in"], s["z_out"], s["z_in"]
+
+    def part(c):
+        return pl.ds(c * rows, rows)
+
+    def along(source, t, c, up):
+        return remote(
+            source,
+            tok.at[t, 0, part(c)],
+            s["zs"].at[0 if up else 1, t, c],
+            s["zr"].at[t, c],
+            above if up else below,
+        )
+
+    def across(source, t, c):
+        return remote(
+            source, tok.at[t, 1, part(c)], s["ys"].at[t, c], s["yr"].at[t, c], beside
+        )
+
+    def spread(source, t, c):
+        @pl.when((t <= z) & (z < LEVELS - 1))
+        def _():
+            along(source, t, c, True).start()
+
+        @pl.when((t >= z) & (z > 0))
+        def _():
+            along(source, t, c, False).start()
+
+        across(source, t, c).start()
+
+    tok[z, 0] = normed[...]
+    for c in range(pieces):
+        spread(normed.at[part(c)], z, c)
+
+    for load in loads[4:]:
+        load.wait()
+    shared_out = s["shared_out"]
+    shared_half = s["sg"].shape[1] // 2
+    for j in range(2):
+        columns = slice(j * shared_half, (j + 1) * shared_half)
+        gate = jnp.dot(normed[...], s["sg"][:, columns], preferred_element_type=f32)
+        upward = jnp.dot(normed[...], s["su"][:, columns], preferred_element_type=f32)
+        s["shared_hidden"][:, columns] = (jax.nn.silu(gate) * upward).astype(bf16)
+
+    def shared_step(k, carry):
+        columns = pl.ds(pl.multiple_of(k * span, span), span)
+        shared_out[:, columns] = mixed[:, columns].astype(f32) + jnp.dot(
+            s["shared_hidden"][...], s["sd"][:, columns], preferred_element_type=f32
+        )
+        return carry
+
+    lax.fori_loop(0, width // span, shared_step, 0)
+
+    for dz, r in peers:
+        route_copy(dz, r, True).wait_recv()
+    for a in range(3):
+        landed(trio(1)[a], s["wtr"].at[a])
+
+    def forward(p):
+        t = level_at(z, p)
+        for c in range(pieces):
+            landed(tok.at[t, 0, part(c)], s["zr"].at[t, c])
+            spread(tok.at[t, 0, part(c)], t, c)
+
+    def relay(a):
+        for k in range(a * WEIGHT_CUTS, (a + 1) * WEIGHT_CUTS):
+            target = trio(2)[a]
+            size = target.shape[0] // WEIGHT_CUTS
+            landed(target.at[pl.ds(k % WEIGHT_CUTS * size, size)], s["wxr"].at[k])
+        core_copy(2, a).start()
+
+    expert_lane = lax.broadcasted_iota(jnp.int32, (count, LANES), 1)
+
+    def scale_column(slot, expert):
+        table = jnp.concatenate(
+            [s["route"][slot], jnp.zeros((LANES - experts, count), f32)], axis=0
+        )
+        picked = jnp.where(expert_lane == expert, jnp.transpose(table), 0.0)
+        return jnp.sum(picked, axis=1, keepdims=True)
+
+    def give(t):
+        for c in range(pieces):
+            y_copy(t, c).start()
+
+    def y_copy(t, c):
+        return remote(
+            y_out.at[t, part(c)], y_in.at[t, part(c)], s["rys"].at[t, c], s["ryr"].at[t, c],
+            beside,
+        )
+
+    hidden = s["hidden"]
+
+    def step(i, carry):
+        p = jnp.where(i < 6, lax.rem(i, 3), 3)
+        e = jnp.where(i < 6, i // 3, i - 6)
+        t = level_at(z, p)
+
+        @pl.when(i == 0)
+        def _():
+            forward(1)
+            forward(2)
+
+        @pl.when(i == 1)
+        def _():
+            forward(3)
+            relay(0)
+
+        @pl.when(i == 2)
+        def _():
+            relay(1)
+
+        @pl.when(i == 3)
+        def _():
+            relay(2)
+            for a in range(3):
+                landed(trio(3)[a], s["wtr"].at[3 + a])
+
+        @pl.when(e == 0)
+        def _():
+            for c in range(pieces):
+                landed(tok.at[t, 1, part(c)], s["yr"].at[t, c])
+
+        expert = jnp.where(e == 0, me, pair)
+        scale = jnp.concatenate(
+            [scale_column(t * 2, expert), scale_column(t * 2 + 1, expert)], axis=0
+        )
+
+        def inner(j, carry):
+            block = tok[t].reshape(2 * count, width)
+            gate = jnp.dot(block, wg[2 * e + j], preferred_element_type=f32)
+            upward = jnp.dot(block, wu[2 * e + j], preferred_element_type=f32)
+            columns = pl.ds(pl.multiple_of(j * half, half), half)
+            hidden[:, columns] = (jax.nn.silu(gate) * upward * scale).astype(bf16)
+            return carry
+
+        lax.fori_loop(0, 2, inner, 0)
+
+        def outer(k, carry):
+            columns = pl.ds(pl.multiple_of(k * span, span), span)
+            depth = pl.ds(pl.multiple_of(e * 2 * half, 2 * half), 2 * half)
+            result = jnp.dot(hidden[...], wd[depth, columns], preferred_element_type=f32)
+
+            @pl.when(e == 0)
+            def _():
+                acc[t, :, columns] = result
+
+            @pl.when(e == 1)
+            def _():
+                whole = acc[t, :, columns] + result
+                acc[t, :, columns] = whole
+                y_out[t, :, columns] = whole[count:].astype(bf16)
+
+            return carry
+
+        lax.fori_loop(0, width // span, outer, 0)
+
+        @pl.when(i == 5)
+        def _():
+            give(level_at(z, 2))
+
+        @pl.when(i == 7)
+        def _():
+            give(level_at(z, 3))
+            give(level_at(z, 1))
+            give(level_at(z, 0))
+
+        return carry
+
+    lax.fori_loop(0, 8, step, 0)
+
+    def take(t, c):
+        landed(y_in.at[t, part(c)], s["ryr"].at[t, c])
+
+    def arrive(slot, c):
+        landed(z_in.at[slot, part(c)], s["rzr"].at[slot, c])
+
+    def hop(p, c):
+        t = level_at(z, p)
+        up = t > z
+        slot = jnp.where(up | (t < z - 1), t, LEVELS)
+        return remote(
+            z_out.at[t, part(c)],
+            z_in.at[slot, part(c)],
+            s["rzs"].at[t, c],
+            s["rzr"].at[slot, c],
+            jnp.where(up, above, below),
+        )
+
+    for p in (2, 3, 1):
+        t = level_at(z, p)
+        up = t > z
+        fed = (up & (z > 0)) | (jnp.logical_not(up) & (z < LEVELS - 1))
+        for c in range(pieces):
+            take(t, c)
+
+            @pl.when(fed)
+            def _():
+                arrive(t, c)
+                z_out[t, part(c)] = (
+                    acc[t, part(c)]
+                    + y_in[t, part(c)].astype(f32)
+                    + z_in[t, part(c)].astype(f32)
+                ).astype(bf16)
+
+            @pl.when(jnp.logical_not(fed))
+            def _():
+                z_out[t, part(c)] = (
+                    acc[t, part(c)] + y_in[t, part(c)].astype(f32)
+                ).astype(bf16)
+
+            hop(p, c).start()
+
+    for c in range(pieces):
+        shared_out[part(c)] += acc[z, part(c)]
+
+        @pl.when(z > 0)
+        def _():
+            arrive(z, c)
+            shared_out[part(c)] += z_in[z, part(c)].astype(f32)
+
+        @pl.when(z < LEVELS - 1)
+        def _():
+            arrive(LEVELS, c)
+            shared_out[part(c)] += z_in[LEVELS, part(c)].astype(f32)
+
+        take(z, c)
+        out_ref[part(c)] = (
+            shared_out[part(c)] + y_in[z, part(c)].astype(f32)
+        ).astype(out_ref.dtype)
+
+    for copy in swaps:
+        copy.wait_send()
+
+    @pl.when(x == 0)
+    def _():
+        query_send(1)[0].wait_send()
+
+    @pl.when(x == 1)
+    def _():
+        query_send(0)[1].wait_send()
+        query_send(1)[1].wait_send()
+        attended_copy(0, 0).wait_send()
+
+    attended_copy(1, 0).wait_send()
+    attended_copy(1, 1).wait_send()
+    attended_copy(0, 1).wait_send()
+    for k in range(3 * WEIGHT_CUTS):
+        weight_piece(k).wait_send()
+    for a in range(3):
+        core_copy(0, a).wait_send()
+        core_copy(2, a).wait_send()
+    for dz, r in peers:
+        route_copy(dz, r, False).wait_send()
+
+    def drain(t, carry):
+        for k in range(2):
+            b = chip(t, y, k)
+
+            @pl.when((t <= z) & (z < LEVELS - 1))
+            def _():
+                kv_along(b, True).wait_send()
+
+            @pl.when((t >= z) & (z > 0))
+            def _():
+                kv_along(b, False).wait_send()
+
+            kv_across(b).wait_send()
+        for c in range(pieces):
+            @pl.when((t <= z) & (z < LEVELS - 1))
+            def _():
+                along(tok.at[t, 0, part(c)], t, c, True).wait_send()
+
+            @pl.when((t >= z) & (z > 0))
+            def _():
+                along(tok.at[t, 0, part(c)], t, c, False).wait_send()
+
+            across(tok.at[t, 0, part(c)], t, c).wait_send()
+            y_copy(t, c).wait_send()
+        return carry
+
+    lax.fori_loop(0, LEVELS, drain, 0)
+    for p in (1, 2, 3):
+        for c in range(pieces):
+            hop(p, c).wait_send()
+
+
+def whole_layer(blocks, vmem_arrays, hbm_arrays, number):
+    count, width = vmem_arrays["residual"].shape
+    tokens = vmem_arrays["query"].shape[0]
+    half = hbm_arrays["gate"].shape[1]
+    middle = hbm_arrays["shared_gate"].shape[1]
+    heads_width = hbm_arrays["project"].shape[0]
+    pieces = 4
+    vmem, hbm = pl.BlockSpec(memory_space=pltpu.VMEM), pl.BlockSpec(memory_space=pl.ANY)
+    bf16, f32 = jnp.bfloat16, jnp.float32
+    dma = pltpu.SemaphoreType.DMA
+    scratch = {
+        "kv": pltpu.VMEM((blocks, 2, tokens, LANES), bf16),
+        "qs": pltpu.VMEM((2, tokens, LANES), bf16),
+        "qm": pltpu.VMEM((2, 2, tokens, LANES), bf16),
+        "after": pltpu.VMEM((tokens, tokens), bf16),
+        "seg": pltpu.VMEM((2, LEVELS, tokens, LANES), f32),
+        "sum": pltpu.VMEM((2, LEVELS, tokens, LANES), f32),
+        "ob": pltpu.VMEM((2, tokens, LANES), bf16),
+        "att": pltpu.VMEM((heads_width // LANES, count, LANES), bf16),
+        "wo": pltpu.VMEM((heads_width, width), bf16),
+        "mixed": pltpu.VMEM((count, width), bf16),
+        "normed": pltpu.VMEM((count, width), bf16),
+        "tok": pltpu.VMEM((LEVELS, 2, count, width), bf16),
+        "acc": pltpu.VMEM((LEVELS, 2 * count, width), f32),
+        "wg": pltpu.VMEM((4, width, half), bf16),
+        "wu": pltpu.VMEM((4, width, half), bf16),
+        "wd": pltpu.VMEM((4 * half, width), bf16),
+        "sg": pltpu.VMEM((width, middle), bf16),
+        "su": pltpu.VMEM((width, middle), bf16),
+        "sd": pltpu.VMEM((middle, width), bf16),
+        "shared_out": pltpu.VMEM((count, width), f32),
+        "hidden": pltpu.VMEM((2 * count, 2 * half), bf16),
+        "shared_hidden": pltpu.VMEM((count, middle), bf16),
+        "y_out": pltpu.VMEM((LEVELS, count, width), bf16),
+        "y_in": pltpu.VMEM((LEVELS, count, width), bf16),
+        "z_out": pltpu.VMEM((LEVELS, count, width), bf16),
+        "z_in": pltpu.VMEM((LEVELS + 1, count, width), bf16),
+        "route": pltpu.VMEM((2 * LEVELS,) + vmem_arrays["table"].shape, f32),
+        "idle": dma((1,)),
+        "load_sem": dma((len(hbm_arrays),)),
+        "near_sem": dma((3,)),
+        "kxs": dma((2,)),
+        "kxr": dma((2,)),
+        "qss": dma((2,)),
+        "qsr": dma((2,)),
+        "kzs": dma((2, blocks)),
+        "kzr": dma((blocks,)),
+        "kys": dma((blocks,)),
+        "kyr": dma((blocks,)),
+        "oss": dma((2, 2)),
+        "osr": dma((4,)),
+        "wts": dma((6,)),
+        "wtr": dma((6,)),
+        "wxs": dma((3 * WEIGHT_CUTS,)),
+        "wxr": dma((3 * WEIGHT_CUTS,)),
+        "w_send": dma((LEVELS, 2)),
+        "w_recv": dma((LEVELS, 2)),
+        "zs": dma((2, LEVELS, pieces)),
+        "zr": dma((LEVELS, pieces)),
+        "ys": dma((LEVELS, pieces)),
+        "yr": dma((LEVELS, pieces)),
+        "rys": dma((LEVELS, pieces)),
+        "ryr": dma((LEVELS, pieces)),
+        "rzs": dma((LEVELS, pieces)),
+        "rzr": dma((LEVELS + 1, pieces)),
+    }
+    names = list(vmem_arrays) + list(hbm_arrays) + ["out"] + list(scratch)
+    return pl.pallas_call(
+        functools.partial(layer_kernel, pieces, names),
+        out_shape=jax.ShapeDtypeStruct((count, width), bf16),
+        in_specs=[vmem] * len(vmem_arrays) + [hbm] * len(hbm_arrays),
+        out_specs=vmem,
+        scratch_shapes=list(scratch.values()),
+        compiler_params=pltpu.CompilerParams(
+            collective_id=number,
+            has_side_effects=True,
+            vmem_limit_bytes=60 * 1024 * 1024,
+        ),
+    )(*vmem_arrays.values(), *hbm_arrays.values())
+
+
 def expert_product(rows, gate_half, up_half, down_half):
     gate = jnp.einsum("seid,edf->seif", rows, gate_half, preferred_element_type=jnp.float32)
     upward = jnp.einsum("seid,edf->seif", rows, up_half, preferred_element_type=jnp.float32)
@@ -231,6 +946,36 @@
     query_count = queries.shape[0]
     local_width = queries.shape[1]
     blocks = lax.axis_size("sp")
+    experts_all = blocks * expert_gate.shape[0]
+    if (
+        blocks == 4 * LEVELS
+        and expert_gate.shape[0] == 1
+        and lax.axis_size("tp") == 2
+        and local_width == 2 * LANES
+    ):
+        picked = routes[:, :, None] == jnp.arange(experts_all, dtype=jnp.int32)
+        table = jnp.sum(jnp.where(picked, route_weight[:, :, None], 0.0), axis=1)
+        return whole_layer(
+            blocks,
+            {
+                "query": queries,
+                "key": key_rows,
+                "value": value_rows,
+                "residual": residual,
+                "gain": norm_gain[None, :],
+                "table": table.T,
+            },
+            {
+                "gate": expert_gate[0],
+                "up": expert_up[0],
+                "down": expert_down[0],
+                "project": out_weight,
+                "shared_gate": shared_gate,
+                "shared_up": shared_up,
+                "shared_down": shared_down,
+            },
+            3,
+        )
     kv = jnp.concatenate([key_rows, value_rows], axis=1)
     kv = gather(kv, blocks, 0).reshape(-1, kv.shape[1])
     attended = attention(queries, kv)

time: 496 us -> 168 us (0.34)
  the two profiles are of different devices: /device:TPU:15 before, /device:TPU:1 now
where the time goes in v2:
time: 168 us; the launch traced here: 167 us
  Pallas kernels  164 us (98%)
  local copies, waits for them, and re-layouts  1.88 us (1%)
    pallas_call x1, Pallas kernels, whole_layer(): pl.pallas_call(functools.partial(layer_kernel, pieces, names), out_shape=...  164 us

profile of v2, /device:TPU:1, one launch (start us, length us, event | category | flops | bytes accessed | tf_op | source)
XLA Modules:
  0.0 167.3 jit_solution(12744281340471678126)
XLA Ops:
  0.0 1.3 select_reduce_fusion
  1.3 164.1 %shard_map.136 = bf16[128,2048]{1,0:T(8,128)(2,1)} custom-call(bf16[256,256]{1,0:T(8,128)(2,1)} %refs_0_.1, bf16[256,256]{1,0:T(8,128)(2,1)} %refs_1_.1, bf16[256,256]{1,0:T(8,128)(2,1)} %refs_2_.1, bf16[128,2048]{1,0:T(8,128)(2,1)} %refs_3_.1, f32[1,2048]{1,0:T(1,128)} %bitcast.9, f32[16,128]{1,0:T(8,128)} %bitcast.8, bf16[2048,256]{1,0:T(8,128)(2,1)} %bitcast.5, ...), custom_call_target="tpu_custom_call" | custom-call | tf_op jit(solution)/shard_map/pallas_call | solution.py:909
  165.4 1.9 %copy.18 = bf16[128,2048]{1,0:T(8,128)(2,1)} copy(bf16[128,2048]{1,0:T(8,128)(2,1)} %shard_map.136) | data formatting | bytes 1048576

commit v3 on v2

--- a/solution.py
+++ b/solution.py
@@ -206,7 +206,10 @@
 
 
 LEVELS = 4
-WEIGHT_CUTS = 4
+FIRST_SHIPPED = 4
+SHIPPED = 11
+SHIP_RATE = 2
+WEIGHT_CUTS = 8
 
 
 def level_at(z, p):
@@ -302,25 +305,36 @@
     query, qs = s["query"], s["qs"]
     kept = pltpu.make_async_copy(query.at[:, lanes(0)], qs.at[0], s["near_sem"].at[2])
 
-    def query_send(place):
-        keep = remote(
+    def query_keep():
+        return remote(
             query.at[:, lanes(1)], qs.at[0], s["qss"].at[1], s["qsr"].at[0], pair
         )
-        move = remote(
+
+    def query_move(place):
+        return remote(
             query.at[:, lanes(place)], qs.at[1], s["qss"].at[place], s["qsr"].at[1],
             mirror + place,
         )
-        return keep, move
 
     @pl.when(x == 0)
     def _():
         kept.start()
-        query_send(1)[0].start()
+        query_keep().start()
 
     @pl.when(x == 1)
     def _():
-        query_send(0)[1].start()
-        query_send(1)[1].start()
+        query_move(0).start()
+        query_move(1).start()
+
+    def weight_piece(k):
+        a, r = k // WEIGHT_CUTS, k % WEIGHT_CUTS
+        source, target = (s["gate"], s["up"], s["down"])[a], trio(2)[a]
+        size = source.shape[0] // WEIGHT_CUTS
+        cut = pl.ds(r * size, size)
+        return remote(source.at[cut], target.at[cut], s["wxs"].at[k], s["wxr"].at[k], pair)
+
+    for k in range(FIRST_SHIPPED):
+        weight_piece(k).start()
 
     def kv_along(b, up):
         return remote(
@@ -360,26 +374,11 @@
         route_copy(dz, r, False).start()
     s["route"][z * 2] = s["table"][...]
 
-    for load in loads[:3]:
-        load.wait()
-
     def core_copy(j, a):
         k = 3 * (j // 2) + a
         return remote(
             trio(j)[a], trio(j + 1)[a], s["wts"].at[k], s["wtr"].at[k], me, 1 - core
         )
-
-    def weight_piece(k):
-        a, r = k // WEIGHT_CUTS, k % WEIGHT_CUTS
-        source, target = trio(0)[a], trio(2)[a]
-        size = source.shape[0] // WEIGHT_CUTS
-        cut = pl.ds(r * size, size)
-        return remote(source.at[cut], target.at[cut], s["wxs"].at[k], s["wxr"].at[k], pair)
-
-    for a in range(3):
-        core_copy(0, a).start()
-    for k in range(2):
-        weight_piece(k).start()
 
     row = lax.broadcasted_iota(jnp.int32, (tokens, tokens), 0)
     column = lax.broadcasted_iota(jnp.int32, (tokens, tokens), 1)
@@ -391,6 +390,23 @@
         landed(kv.at[pair, k], s["kxr"].at[k])
     kv_spread(pair)
 
+    def kv_forward(p, mine):
+        b = chip(level_at(z, p), y, x if mine else 1 - x)
+        landed(kv.at[b], s["kzr"].at[b])
+        kv_spread(b)
+
+    edge = (z == 0) | (z == LEVELS - 1)
+    inner_level = jnp.logical_not(edge)
+    kv_forward(1, True)
+
+    @pl.when(inner_level)
+    def _():
+        kv_forward(2, True)
+
+    for load in loads[:3]:
+        load.wait()
+    for a in range(3):
+        core_copy(0, a).start()
     @pl.when(x == 0)
     def _():
         kept.wait()
@@ -406,13 +422,6 @@
         scaled = qs[f].astype(f32) * HEAD_DIM ** (-0.5)
         s["qm"][f, 0] = jnp.where(first, scaled, 0.0).astype(bf16)
         s["qm"][f, 1] = jnp.where(first, 0.0, scaled).astype(bf16)
-
-    def kv_forward(p):
-        t = level_at(z, p)
-        for k in range(2):
-            b = chip(t, y, k)
-            landed(kv.at[b], s["kzr"].at[b])
-            kv_spread(b)
 
     def tile(f, t, b, diagonal):
         parts, totals = [], []
@@ -441,61 +450,67 @@
         s["sum"][f, t] += total
 
     kept_block = chip(z, y, 0)
+    order = ((0, 0), (0, 1), (1, 0), (2, 0), (1, 1), (3, 0), (2, 1), (3, 1))
 
     def attend(i, carry):
-        @pl.when(i == 0)
-        def _():
-            kv_forward(1)
-            kv_forward(2)
+        p = functools.reduce(lambda a, k: jnp.where(i == k, order[k][0], a), range(1, 8), 0)
+        far = functools.reduce(lambda a, k: jnp.where(i == k, order[k][1], a), range(1, 8), 0)
 
         @pl.when(i == 1)
         def _():
-            kv_forward(3)
-
-        t = level_at(z, i)
-        for k in range(2):
-            b = chip(t, 1 - y, k)
-            landed(kv.at[b], s["kyr"].at[b])
+            kv_forward(1, False)
+
+        for at, far_level, mine in ((1, 2, True), (2, 2, False), (3, 3, True), (4, 3, False)):
+            @pl.when((i == at) & edge)
+            def _():
+                kv_forward(far_level, mine)
+
+        for at, far_level, mine in ((1, 2, False), (2, 3, True), (3, 3, False)):
+            @pl.when((i == at) & inner_level)
+            def _():
+                kv_forward(far_level, mine)
+
+        t = level_at(z, p)
+        side = jnp.where(far == 1, 1 - y, y)
+        start = chip(t, side, 0)
+        segment = start // 2
+
+        @pl.when(far == 1)
+        def _():
+            for k in range(2):
+                landed(kv.at[start + k], s["kyr"].at[start + k])
 
         def one_query(f, carry):
             block = jnp.where(f == 0, kept_block, blocks - 1 - kept_block)
-            full = jnp.clip(block - 4 * t, 0, 4)
+            full = jnp.clip(block - start, 0, 2)
 
             def one_key(b, carry):
-                tile(f, t, 4 * t + b, False)
+                tile(f, segment, start + b, False)
                 return carry
 
             lax.fori_loop(0, full, one_key, 0)
 
-            @pl.when((block >= 4 * t) & (block < 4 * t + 4))
-            def _():
-                tile(f, t, block, True)
+            @pl.when((block >= start) & (block < start + 2))
+            def _():
+                tile(f, segment, block, True)
 
             return carry
 
         lax.fori_loop(0, 2, one_query, 0)
 
-        @pl.when(i == 0)
-        def _():
-            weight_piece(2).start()
-            weight_piece(3).start()
-
-        @pl.when(i == 1)
-        def _():
-            weight_piece(4).start()
-
-        @pl.when(i == 2)
-        def _():
-            weight_piece(5).start()
+        for k in range(FIRST_SHIPPED, SHIPPED):
+            @pl.when(i == (k - FIRST_SHIPPED) // SHIP_RATE)
+            def _():
+                weight_piece(k).start()
 
         return carry
 
-    lax.fori_loop(0, LEVELS, attend, 0)
+    lax.fori_loop(0, 2 * LEVELS, attend, 0)
 
     for f in range(2):
-        later = s["sum"][f, LEVELS - 1]
-        value = s["seg"][f, LEVELS - 1]
-        for t in reversed(range(LEVELS - 1)):
+        later = s["sum"][f, 2 * LEVELS - 1]
+        value = s["seg"][f, 2 * LEVELS - 1]
+        for t in reversed(range(2 * LEVELS - 1)):
             value = value + jnp.exp(-later) * s["seg"][f, t]
             later = later + s["sum"][f, t]
         s["ob"][f] = value.astype(bf16)
@@ -528,7 +543,7 @@
         def _():
             landed(s["att"].at[k], s["osr"].at[k])
 
-    for k in range(6, 3 * WEIGHT_CUTS):
+    for k in range(SHIPPED, 3 * WEIGHT_CUTS):
         weight_piece(k).start()
 
     mixed, normed = s["mixed"], s["normed"]
@@ -646,8 +661,8 @@
     hidden = s["hidden"]
 
     def step(i, carry):
-        p = jnp.where(i < 6, lax.rem(i, 3), 3)
-        e = jnp.where(i < 6, i // 3, i - 6)
+        p = jnp.where(i < 3, i, jnp.where(i == 3, 2, jnp.where(i < 6, 3, 7 - i)))
+        e = ((i == 3) | (i > 4)).astype(jnp.int32)
         t = level_at(z, p)
 
         @pl.when(i == 0)
@@ -655,9 +670,12 @@
             forward(1)
             forward(2)
 
+        @pl.when(((i == 1) & jnp.logical_not(edge)) | ((i == 2) & edge))
+        def _():
+            forward(3)
+
         @pl.when(i == 1)
         def _():
-            forward(3)
             relay(0)
 
         @pl.when(i == 2)
@@ -709,15 +727,9 @@
 
         lax.fori_loop(0, width // span, outer, 0)
 
-        @pl.when(i == 5)
-        def _():
-            give(level_at(z, 2))
-
-        @pl.when(i == 7)
-        def _():
-            give(level_at(z, 3))
-            give(level_at(z, 1))
-            give(level_at(z, 0))
+        @pl.when(e == 1)
+        def _():
+            give(t)
 
         return carry
 
@@ -788,12 +800,12 @@
 
     @pl.when(x == 0)
     def _():
-        query_send(1)[0].wait_send()
+        query_keep().wait_send()
 
     @pl.when(x == 1)
     def _():
-        query_send(0)[1].wait_send()
-        query_send(1)[1].wait_send()
+        query_move(0).wait_send()
+        query_move(1).wait_send()
         attended_copy(0, 0).wait_send()
 
     attended_copy(1, 0).wait_send()
@@ -854,8 +866,8 @@
         "qs": pltpu.VMEM((2, tokens, LANES), bf16),
         "qm": pltpu.VMEM((2, 2, tokens, LANES), bf16),
         "after": pltpu.VMEM((tokens, tokens), bf16),
-        "seg": pltpu.VMEM((2, LEVELS, tokens, LANES), f32),
-        "sum": pltpu.VMEM((2, LEVELS, tokens, LANES), f32),
+        "seg": pltpu.VMEM((2, 2 * LEVELS, tokens, LANES), f32),
+        "sum": pltpu.VMEM((2, 2 * LEVELS, tokens, LANES), f32),
         "ob": pltpu.VMEM((2, tokens, LANES), bf16),
         "att": pltpu.VMEM((heads_width // LANES, count, LANES), bf16),
         "wo": pltpu.VMEM((heads_width, width), bf16),

time: 168 us -> 154 us (0.917)
  the two profiles are of different devices: /device:TPU:1 before, /device:TPU:15 now
where the time goes in v3:
time: 154 us; the launch traced here: 151 us
  Pallas kernels  148 us (96%)
  local copies, waits for them, and re-layouts  1.88 us (1%)
    pallas_call x1, Pallas kernels, whole_layer(): pl.pallas_call(functools.partial(layer_kernel, pieces, names), out_shape=...  148 us

profile of v3, /device:TPU:15, one launch (start us, length us, event | category | flops | bytes accessed | tf_op | source)
XLA Modules:
  0.0 151.4 jit_solution(2937769094790607594)
XLA Ops:
  0.0 1.3 select_reduce_fusion
  1.3 148.2 %shard_map.136 = bf16[128,2048]{1,0:T(8,128)(2,1)} custom-call(bf16[256,256]{1,0:T(8,128)(2,1)} %refs_0_.1, bf16[256,256]{1,0:T(8,128)(2,1)} %refs_1_.1, bf16[256,256]{1,0:T(8,128)(2,1)} %refs_2_.1, bf16[128,2048]{1,0:T(8,128)(2,1)} %refs_3_.1, f32[1,2048]{1,0:T(1,128)} %bitcast.9, f32[16,128]{1,0:T(8,128)} %bitcast.8, bf16[2048,256]{1,0:T(8,128)(2,1)} %bitcast.5, ...), custom_call_target="tpu_custom_call" | custom-call | tf_op jit(solution)/shard_map/pallas_call | solution.py:921
  149.5 1.9 %copy.18 = bf16[128,2048]{1,0:T(8,128)(2,1)} copy(bf16[128,2048]{1,0:T(8,128)(2,1)} %shard_map.136) | data formatting | bytes 1048576

commit v4 on v3

--- a/solution.py
+++ b/solution.py
@@ -206,6 +206,7 @@
 
 
 LEVELS = 4
+EARLY_PIECES = 2
 FIRST_SHIPPED = 4
 SHIPPED = 11
 SHIP_RATE = 2
@@ -280,6 +281,20 @@
     for copy in near:
         copy.start()
 
+    name = lax.broadcasted_iota(jnp.int32, (experts, count), 0)
+    table = jnp.zeros((experts, count), f32)
+    for k in range(s["chosen"].shape[0]):
+        mine = s["chosen"][k : k + 1] == name
+        table = table + jnp.where(mine, s["chosen_weight"][k : k + 1], 0.0)
+    s["table"][...] = table
+    s["route"][z * 2] = table
+    row = lax.broadcasted_iota(jnp.int32, (tokens, tokens), 0)
+    column = lax.broadcasted_iota(jnp.int32, (tokens, tokens), 1)
+    for k in range(2):
+        s["after"][k * tokens : (k + 1) * tokens] = (row > column).astype(bf16)
+    s["seg"][...] = jnp.zeros_like(s["seg"])
+    s["sum"][...] = jnp.zeros_like(s["sum"])
+
     barrier = pltpu.get_barrier_semaphore()
     peers = [(dz, r) for dz in range(LEVELS) for r in range(2) if (dz, r) != (0, 0)]
     greeted = [
@@ -372,7 +387,6 @@
 
     for dz, r in peers:
         route_copy(dz, r, False).start()
-    s["route"][z * 2] = s["table"][...]
 
     def core_copy(j, a):
         k = 3 * (j // 2) + a
@@ -380,11 +394,6 @@
             trio(j)[a], trio(j + 1)[a], s["wts"].at[k], s["wtr"].at[k], me, 1 - core
         )
 
-    row = lax.broadcasted_iota(jnp.int32, (tokens, tokens), 0)
-    column = lax.broadcasted_iota(jnp.int32, (tokens, tokens), 1)
-    s["after"][...] = (row > column).astype(bf16)
-    s["seg"][...] = jnp.zeros_like(s["seg"])
-    s["sum"][...] = jnp.zeros_like(s["sum"])
 
     for k in range(2):
         landed(kv.at[pair, k], s["kxr"].at[k])
@@ -438,8 +447,10 @@
                 cost = jnp.where(mask, cost, 0.0)
             high = cost.astype(bf16)
             low = (cost - high.astype(f32)).astype(bf16)
-            inside = jnp.dot(high, s["after"][...], preferred_element_type=f32)
-            inside = inside + jnp.dot(low, s["after"][...], preferred_element_type=f32)
+            inside = jnp.dot(
+                jnp.concatenate([high, low], axis=1), s["after"][...],
+                preferred_element_type=f32,
+            )
             weight = jnp.exp(jnp.minimum(scores, 0.0) - tail - inside)
             if diagonal:
                 weight = jnp.where(mask, weight, 0.0)
@@ -659,81 +670,6 @@
         )
 
     hidden = s["hidden"]
-
-    def step(i, carry):
-        p = jnp.where(i < 3, i, jnp.where(i == 3, 2, jnp.where(i < 6, 3, 7 - i)))
-        e = ((i == 3) | (i > 4)).astype(jnp.int32)
-        t = level_at(z, p)
-
-        @pl.when(i == 0)
-        def _():
-            forward(1)
-            forward(2)
-
-        @pl.when(((i == 1) & jnp.logical_not(edge)) | ((i == 2) & edge))
-        def _():
-            forward(3)
-
-        @pl.when(i == 1)
-        def _():
-            relay(0)
-
-        @pl.when(i == 2)
-        def _():
-            relay(1)
-
-        @pl.when(i == 3)
-        def _():
-            relay(2)
-            for a in range(3):
-                landed(trio(3)[a], s["wtr"].at[3 + a])
-
-        @pl.when(e == 0)
-        def _():
-            for c in range(pieces):
-                landed(tok.at[t, 1, part(c)], s["yr"].at[t, c])
-
-        expert = jnp.where(e == 0, me, pair)
-        scale = jnp.concatenate(
-            [scale_column(t * 2, expert), scale_column(t * 2 + 1, expert)], axis=0
-        )
-
-        def inner(j, carry):
-            block = tok[t].reshape(2 * count, width)
-            gate = jnp.dot(block, wg[2 * e + j], preferred_element_type=f32)
-            upward = jnp.dot(block, wu[2 * e + j], preferred_element_type=f32)
-            columns = pl.ds(pl.multiple_of(j * half, half), half)
-            hidden[:, columns] = (jax.nn.silu(gate) * upward * scale).astype(bf16)
-            return carry
-
-        lax.fori_loop(0, 2, inner, 0)
-
-        def outer(k, carry):
-            columns = pl.ds(pl.multiple_of(k * span, span), span)
-            depth = pl.ds(pl.multiple_of(e * 2 * half, 2 * half), 2 * half)
-            result = jnp.dot(hidden[...], wd[depth, columns], preferred_element_type=f32)
-
-            @pl.when(e == 0)
-            def _():
-                acc[t, :, columns] = result
-
-            @pl.when(e == 1)
-            def _():
-                whole = acc[t, :, columns] + result
-                acc[t, :, columns] = whole
-                y_out[t, :, columns] = whole[count:].astype(bf16)
-
-            return carry
-
-        lax.fori_loop(0, width // span, outer, 0)
-
-        @pl.when(e == 1)
-        def _():
-            give(t)
-
-        return carry
-
-    lax.fori_loop(0, 8, step, 0)
 
     def take(t, c):
         landed(y_in.at[t, part(c)], s["ryr"].at[t, c])
@@ -753,29 +689,124 @@
             jnp.where(up, above, below),
         )
 
-    for p in (2, 3, 1):
+    def combine(p, c):
         t = level_at(z, p)
         up = t > z
         fed = (up & (z > 0)) | (jnp.logical_not(up) & (z < LEVELS - 1))
+        take(t, c)
+
+        @pl.when(fed)
+        def _():
+            arrive(t, c)
+            z_out[t, part(c)] = (
+                acc[t, part(c)]
+                + y_in[t, part(c)].astype(f32)
+                + z_in[t, part(c)].astype(f32)
+            ).astype(bf16)
+
+        @pl.when(jnp.logical_not(fed))
+        def _():
+            z_out[t, part(c)] = (
+                acc[t, part(c)] + y_in[t, part(c)].astype(f32)
+            ).astype(bf16)
+
+        hop(p, c).start()
+
+    def step(i, carry):
+        p = jnp.where(i < 3, i, jnp.where(i == 3, 2, jnp.where(i < 6, 3, 7 - i)))
+        e = ((i == 3) | (i > 4)).astype(jnp.int32)
+        t = level_at(z, p)
+
+        @pl.when(i == 0)
+        def _():
+            forward(1)
+            forward(2)
+
+        @pl.when(((i == 1) & jnp.logical_not(edge)) | ((i == 2) & edge))
+        def _():
+            forward(3)
+
+        @pl.when(i == 1)
+        def _():
+            relay(0)
+
+        @pl.when(i == 2)
+        def _():
+            relay(1)
+
+        @pl.when(i == 3)
+        def _():
+            relay(2)
+            for a in range(3):
+                landed(trio(3)[a], s["wtr"].at[3 + a])
+
+        @pl.when(i == 6)
+        def _():
+            for c in range(EARLY_PIECES // 2):
+                combine(2, c)
+
+        @pl.when(i == 7)
+        def _():
+            for c in range(EARLY_PIECES // 2, EARLY_PIECES):
+                combine(2, c)
+
+        @pl.when(e == 0)
+        def _():
+            for c in range(pieces):
+                landed(tok.at[t, 1, part(c)], s["yr"].at[t, c])
+
+        expert = jnp.where(e == 0, me, pair)
+        scale = jnp.concatenate(
+            [scale_column(t * 2, expert), scale_column(t * 2 + 1, expert)], axis=0
+        )
+
+        def inner(j, carry):
+            block = tok[t].reshape(2 * count, width)
+            gate = jnp.dot(block, wg[2 * e + j], preferred_element_type=f32)
+            upward = jnp.dot(block, wu[2 * e + j], preferred_element_type=f32)
+            columns = pl.ds(pl.multiple_of(j * half, half), half)
+            hidden[:, columns] = (jax.nn.silu(gate) * upward * scale).astype(bf16)
+            return carry
+
+        lax.fori_loop(0, 2, inner, 0)
+
+        def outer(k, carry):
+            columns = pl.ds(pl.multiple_of(k * span, span), span)
+            depth = pl.ds(pl.multiple_of(e * 2 * half, 2 * half), 2 * half)
+            result = jnp.dot(hidden[...], wd[depth, columns], preferred_element_type=f32)
+
+            @pl.when(e == 0)
+            def _():
+                acc[t, :, columns] = result
+
+            @pl.when(e == 1)
+            def _():
+                whole = acc[t, :, columns] + result
+                acc[t, :, columns] = whole
+                y_out[t, :, columns] = whole[count:].astype(bf16)
+
+            return carry
+
+        lax.fori_loop(0, width // span, outer, 0)
+
+        @pl.when(e == 1)
+        def _():
+            give(t)
+
+        return carry
+
+    lax.fori_loop(0, 8, step, 0)
+
+    for c in range(EARLY_PIECES, pieces):
+        combine(2, c)
+    for p in (3, 1):
         for c in range(pieces):
-            take(t, c)
-
-            @pl.when(fed)
-            def _():
-                arrive(t, c)
-                z_out[t, part(c)] = (
-                    acc[t, part(c)]
-                    + y_in[t, part(c)].astype(f32)
-                    + z_in[t, part(c)].astype(f32)
-                ).astype(bf16)
-
-            @pl.when(jnp.logical_not(fed))
-            def _():
-                z_out[t, part(c)] = (
-                    acc[t, part(c)] + y_in[t, part(c)].astype(f32)
-                ).astype(bf16)
-
-            hop(p, c).start()
+            combine(p, c)
+
+    def stage_copy(c):
+        return pltpu.make_async_copy(
+            s["stage"].at[part(c)], out_ref.at[part(c)], s["stage_sem"].at[c]
+        )
 
     for c in range(pieces):
         shared_out[part(c)] += acc[z, part(c)]
@@ -791,10 +822,13 @@
             shared_out[part(c)] += z_in[LEVELS, part(c)].astype(f32)
 
         take(z, c)
-        out_ref[part(c)] = (
+        s["stage"][part(c)] = (
             shared_out[part(c)] + y_in[z, part(c)].astype(f32)
-        ).astype(out_ref.dtype)
-
+        ).astype(bf16)
+        stage_copy(c).start()
+
+    for c in range(pieces):
+        stage_copy(c).wait()
     for copy in swaps:
         copy.wait_send()
 
@@ -865,7 +899,8 @@
         "kv": pltpu.VMEM((blocks, 2, tokens, LANES), bf16),
         "qs": pltpu.VMEM((2, tokens, LANES), bf16),
         "qm": pltpu.VMEM((2, 2, tokens, LANES), bf16),
-        "after": pltpu.VMEM((tokens, tokens), bf16),
+        "after": pltpu.VMEM((2 * tokens, tokens), bf16),
+        "table": pltpu.VMEM((blocks, count), f32),
         "seg": pltpu.VMEM((2, 2 * LEVELS, tokens, LANES), f32),
         "sum": pltpu.VMEM((2, 2 * LEVELS, tokens, LANES), f32),
         "ob": pltpu.VMEM((2, tokens, LANES), bf16),
@@ -888,7 +923,9 @@
         "y_in": pltpu.VMEM((LEVELS, count, width), bf16),
         "z_out": pltpu.VMEM((LEVELS, count, width), bf16),
         "z_in": pltpu.VMEM((LEVELS + 1, count, width), bf16),
-        "route": pltpu.VMEM((2 * LEVELS,) + vmem_arrays["table"].shape, f32),
+        "route": pltpu.VMEM((2 * LEVELS, blocks, count), f32),
+        "stage": pltpu.VMEM((count, width), bf16),
+        "stage_sem": dma((pieces,)),
         "idle": dma((1,)),
         "load_sem": dma((len(hbm_arrays),)),
         "near_sem": dma((3,)),
@@ -922,7 +959,7 @@
         functools.partial(layer_kernel, pieces, names),
         out_shape=jax.ShapeDtypeStruct((count, width), bf16),
         in_specs=[vmem] * len(vmem_arrays) + [hbm] * len(hbm_arrays),
-        out_specs=vmem,
+        out_specs=hbm,
         scratch_shapes=list(scratch.values()),
         compiler_params=pltpu.CompilerParams(
             collective_id=number,
@@ -965,8 +1002,6 @@
         and lax.axis_size("tp") == 2
         and local_width == 2 * LANES
     ):
-        picked = routes[:, :, None] == jnp.arange(experts_all, dtype=jnp.int32)
-        table = jnp.sum(jnp.where(picked, route_weight[:, :, None], 0.0), axis=1)
         return whole_layer(
             blocks,
             {
@@ -975,7 +1010,8 @@
                 "value": value_rows,
                 "residual": residual,
                 "gain": norm_gain[None, :],
-                "table": table.T,
+                "chosen": routes.T,
+                "chosen_weight": route_weight.T,
             },
             {
                 "gate": expert_gate[0],

time: 154 us -> 149 us (0.968)
  the two profiles are of different devices: /device:TPU:15 before, /device:TPU:3 now
where the time goes in v4:
time: 149 us
  Pallas kernels  147 us (99%)
  local copies, waits for them, and re-layouts  1.88 us (1%)
    pallas_call x1, Pallas kernels, whole_layer(): pl.pallas_call(functools.partial(layer_kernel, pieces, names), out_shape=...  147 us

profile of v4, /device:TPU:3, one launch (start us, length us, event | category | flops | bytes accessed | tf_op | source)
XLA Modules:
  0.0 148.8 jit_solution(15185584998829935260)
XLA Ops:
  0.0 146.9 %shard_map.136 = bf16[128,2048]{1,0:T(8,128)(2,1)} custom-call(bf16[256,256]{1,0:T(8,128)(2,1)} %refs_0_.1, bf16[256,256]{1,0:T(8,128)(2,1)} %refs_1_.1, bf16[256,256]{1,0:T(8,128)(2,1)} %refs_2_.1, bf16[128,2048]{1,0:T(8,128)(2,1)} %refs_3_.1, f32[1,2048]{1,0:T(1,128)} %bitcast.9, s32[8,128]{1,0:T(8,128)} %bitcast.10, f32[8,128]{1,0:T(8,128)} %bitcast.11, ...), custom_call_target="tpu_custom_call" | custom-call | tf_op jit(solution)/shard_map/pallas_call | solution.py:958
  146.9 1.9 %copy.16 = bf16[128,2048]{1,0:T(8,128)(2,1)} copy(bf16[128,2048]{1,0:T(8,128)(2,1)} %shard_map.136) | data formatting | bytes 1048576
